TPU v7x, 32 devices: a whole 2x2x4 slice. The times are simulated.
32 devices in a mesh: ep: 16 (over z, y, x), tp: 2 (over core).
Axes of the slice: x: 2, y: 2, z: 4, core: 2. Of those that a mesh axis runs over, the one named last changes fastest.
Arguments:
- tokens: bfloat16 [256, 2048], P('ep'), may hold values from -6 to 6
- recurrent_state: float32 [256, 4, 128, 256], P('ep', 'tp'), may hold values from -6 to 6
- query_weight: bfloat16 [2048, 512], P(None, 'tp'), may hold values from -0.125 to 0.125
- key_weight: bfloat16 [2048, 512], P(None, 'tp'), may hold values from -0.125 to 0.125
- decay_weight: bfloat16 [2048, 512], P(None, 'tp'), may hold values from -0.5 to 0.5
- value_weight: bfloat16 [2048, 1024], P(None, 'tp'), may hold values from -0.125 to 0.125
- gate_weight: bfloat16 [2048, 1024], P(None, 'tp'), may hold values from -0.125 to 0.125
- head_gain: float32 [256], replicated, may hold values from 0.1 to 1.9
- output_weight: bfloat16 [1024, 2048], P('tp'), may hold values from -0.375 to 0.375
- norm_gain: float32 [2, 2048], replicated, may hold values from 0.1 to 1.9
- norm_bias: float32 [2, 2048], replicated, may hold values from -1.8 to 1.8
- group_router: bfloat16 [2048, 4], replicated, may hold values from -0.125 to 0.125
- router_weight: bfloat16 [2048, 32], replicated, may hold values from -0.125 to 0.125
- routes: int32 [256, 2], P('ep'), may hold values from 0 to 31, as said below
- expert_gate: bfloat16 [32, 2048, 256], P(('ep', 'tp')), may hold values from -0.125 to 0.125
- expert_up: bfloat16 [32, 2048, 256], P(('ep', 'tp')), may hold values from -0.125 to 0.125
- expert_down: bfloat16 [32, 256, 2048], P(('ep', 'tp')), may hold values from -1.5 to 1.5
Outputs:
- new_tokens: bfloat16 [256, 2048], P('ep', 'tp')
- new_state: float32 [256, 4, 128, 256], P('ep', 'tp')
Inputs may be any that keep to these rules, and one draw needn't show every extreme that they name: `routes`: each row names two different experts of one group (group g holds the experts g * 8 to g * 8 + 7). In the rows of one device each group is named by the same number of rows and no expert by more than 2 rows; some expert is named by exactly 2 rows of every device.
All inputs are finite; a program needn't handle non-finite values.
Results may differ from a plain program's by a relative error of at most 0.01.
Values may be sent and summed in bfloat16 or wider, within the bound.
No kernel may reach another device: no remote copies, remote signals or barrier semaphores. Data moves between devices by JAX's collectives and lax.ppermute only.
A program may use at most 128 MiB of HBM per device.

v0:
```python
import jax
import jax.numpy as jnp
from jax import lax
from jax.sharding import PartitionSpec as P

alpha_res = 2.0**0.5
eps_norm = 1e-05


def layer_normed(inputs, gain_row, bias_row):
    centered = inputs - jnp.mean(inputs, axis=-1, keepdims=True)
    spread = jnp.mean(centered * centered, axis=-1, keepdims=True)
    return centered * lax.rsqrt(spread + eps_norm) * gain_row + bias_row


def on_device(
    tokens,
    recurrent_state,
    query_weight,
    key_weight,
    decay_weight,
    value_weight,
    gate_weight,
    head_gain,
    output_weight,
    norm_gain,
    norm_bias,
    group_router,
    router_weight,
    routes,
    expert_gate,
    expert_up,
    expert_down,
):
    row_count, model_width = tokens.shape
    heads_here = recurrent_state.shape[1]
    key_dim = recurrent_state.shape[2]
    value_dim = recurrent_state.shape[3]

    def project(weight):
        return jnp.dot(tokens, weight, preferred_element_type=jnp.float32)

    queries = project(query_weight).reshape(row_count, heads_here, key_dim) * key_dim ** (-0.5)
    key_rows = project(key_weight).reshape(row_count, heads_here, key_dim)
    value_rows = project(value_weight).reshape(row_count, heads_here, value_dim)
    gate_rows = project(gate_weight)
    decay_rate = jnp.exp(jax.nn.log_sigmoid(project(decay_weight)) / 16.0).reshape(
        row_count, heads_here, key_dim
    )
    new_state = (
        decay_rate[..., None] * recurrent_state + key_rows[..., None] * value_rows[:, :, None, :]
    )
    readout = jnp.sum(queries[..., None] * new_state, axis=2)
    norm_scale = lax.rsqrt(jnp.mean(readout * readout, axis=-1, keepdims=True) + eps_norm)
    gated_rows = (
        (readout * norm_scale * head_gain).reshape(row_count, heads_here * value_dim)
        * jax.nn.silu(gate_rows)
    ).astype(jnp.bfloat16)
    partial_value = jnp.dot(gated_rows, output_weight, preferred_element_type=jnp.float32)
    mixed_sum = lax.psum(partial_value.astype(jnp.bfloat16), "tp").astype(jnp.float32)
    hidden = layer_normed(
        alpha_res * tokens.astype(jnp.float32) + mixed_sum, norm_gain[0], norm_bias[0]
    ).astype(jnp.bfloat16)
    group_count = group_router.shape[1]
    expert_count = router_weight.shape[1]
    per_group = expert_count // group_count
    top_count = routes.shape[1]
    group_logit = jnp.dot(hidden, group_router, preferred_element_type=jnp.float32)
    expert_logit = jnp.dot(hidden, router_weight, preferred_element_type=jnp.float32)
    chosen_group = routes[:, 0] // per_group
    group_hit = chosen_group[:, None] == jnp.arange(group_count, dtype=jnp.int32)[None, :]
    own_logit = jnp.sum(jnp.where(group_hit, group_logit, 0.0), axis=1, keepdims=True)
    group_share = 1.0 / jnp.sum(jnp.exp(group_logit - own_logit), axis=1)
    expert_hit = routes[:, :, None] == jnp.arange(expert_count, dtype=jnp.int32)[None, None, :]
    picked = jnp.sum(jnp.where(expert_hit, expert_logit[:, None, :], 0.0), axis=2)
    route_weight = group_share[:, None] * jax.nn.sigmoid(picked - picked[:, ::-1])
    ep_count = lax.axis_size("ep")
    tp_count = lax.axis_size("tp")
    pair_index = lax.axis_index("tp")
    local_experts = expert_gate.shape[0]
    capacity = 2 * max(1, row_count // expert_count)
    total_slots = expert_count * capacity
    own_slots = total_slots // tp_count
    flat_routes = routes.reshape(row_count * top_count)
    onehot = (flat_routes[:, None] == jnp.arange(expert_count, dtype=jnp.int32)[None, :]).astype(
        jnp.int32
    )
    earlier_count = jnp.sum((jnp.cumsum(onehot, axis=0) - onehot) * onehot, axis=1)
    slot_index = flat_routes * capacity + earlier_count
    pick_all = (slot_index[:, None] == jnp.arange(total_slots, dtype=jnp.int32)[None, :]).astype(
        jnp.bfloat16
    )
    pick_mine = lax.dynamic_slice_in_dim(
        pick_all.reshape(row_count * top_count, ep_count, tp_count, local_experts * capacity),
        pair_index,
        1,
        2,
    ).reshape(row_count * top_count, own_slots)
    outgoing = jnp.einsum(
        "rks,rd->sd",
        pick_mine.reshape(row_count, top_count, own_slots),
        hidden,
        preferred_element_type=jnp.float32,
    ).astype(jnp.bfloat16)
    outgoing = outgoing.reshape(ep_count, local_experts, capacity, model_width)
    col_width = model_width // tp_count
    col_start = pair_index * col_width
    arrived = lax.all_to_all(outgoing, "ep", split_axis=0, concat_axis=0, tiled=True)
    gate_part = jnp.einsum(
        "secd,edf->secf", arrived, expert_gate, preferred_element_type=jnp.float32
    )
    up_part = jnp.einsum("secd,edf->secf", arrived, expert_up, preferred_element_type=jnp.float32)
    activation = (jax.nn.silu(gate_part) * up_part).astype(jnp.bfloat16)
    results = jnp.einsum(
        "secf,efd->secd", activation, expert_down, preferred_element_type=jnp.float32
    ).astype(jnp.bfloat16)
    returned = lax.all_to_all(
        lax.all_to_all(results, "ep", split_axis=0, concat_axis=0, tiled=True),
        "tp",
        split_axis=3,
        concat_axis=1,
        tiled=True,
    )
    fetched = jnp.dot(
        pick_all, returned.reshape(total_slots, col_width), preferred_element_type=jnp.float32
    ).reshape(row_count, top_count, col_width)
    routed_sum = jnp.sum(route_weight[..., None] * fetched, axis=1)
    blended = (
        alpha_res * lax.dynamic_slice_in_dim(hidden, col_start, col_width, 1).astype(jnp.float32)
        + routed_sum
    )
    row_total, row_squares = lax.psum(
        (jnp.sum(blended, axis=1), jnp.sum(blended * blended, axis=1)), "tp"
    )
    row_mean = row_total / model_width
    spread = row_squares / model_width - row_mean * row_mean
    gain_part = lax.dynamic_slice_in_dim(norm_gain[1], col_start, col_width, 0)
    shift_part = lax.dynamic_slice_in_dim(norm_bias[1], col_start, col_width, 0)
    new_tokens = (
        (blended - row_mean[:, None]) * lax.rsqrt(spread[:, None] + eps_norm) * gain_part
        + shift_part
    ).astype(jnp.bfloat16)
    return (new_tokens, new_state)


def solution(mesh):
    in_specs = (
        P("ep", None),
        P("ep", "tp", None, None),
        P(None, "tp"),
        P(None, "tp"),
        P(None, "tp"),
        P(None, "tp"),
        P(None, "tp"),
        P(),
        P("tp", None),
        P(),
        P(),
        P(),
        P(),
        P("ep", None),
        P(("ep", "tp"), None, None),
        P(("ep", "tp"), None, None),
        P(("ep", "tp"), None, None),
    )
    out_specs = (P("ep", "tp"), P("ep", "tp", None, None))
    return jax.shard_map(
        on_device, mesh=mesh, in_specs=in_specs, out_specs=out_specs, check_vma=False
    )
```

profile of v0, /device:TPU:0, one launch (start us, length us, event | category | flops | bytes accessed | tf_op | source)
XLA Modules:
  0.0 94.1 jit_solution(932960176985230560)
XLA Ops:
  7.2 0.0 copy-start
  7.2 0.0 all-reduce.3.cloned.1.call-start
  7.2 1.7 %convolution_multiply_fusion.1 = f32[16,256]{1,0:T(8,128)S(1)} fusion(bf16[16,2048]{1,0:T(8,128)(2,1)} %param.17, bf16[2048,256]{1,0:T(8,128)(2,1)} %param.19), kind=kOutput, calls=%fused_computation.14 | convolution fusion | flops 16781312 | bytes 1130496 | tf_op jit(solution)/shard_map/dot_general | solution.py:41
  8.9 2.0 %fusion.42 = f32[16,512]{1,0:T(8,128)S(1)} fusion(bf16[16,2048]{1,0:T(8,128)(2,1)} %param.17, bf16[2048,512]{1,0:T(8,128)(2,1)} %param.22), kind=kOutput, calls=%fused_computation.83 | convolution fusion | flops 33554432 | bytes 2195456 | tf_op jit(solution)/shard_map/dot_general | solution.py:41
  11.0 0.2 fusion.41
  11.3 1.5 %fusion.25 = f32[16,256]{1,0:T(8,128)S(1)} fusion(bf16[16,2048]{1,0:T(8,128)(2,1)S(1)} %copy-done.1, bf16[2048,256]{1,0:T(8,128)(2,1)} %param.21), kind=kOutput, calls=%fused_computation.41 | convolution fusion | flops 16814080 | bytes 1130496 | tf_op jit(solution)/shard_map/dot_general | solution.py:41
  12.8 5.7 %multiply_reduce_fusion = (f32[16,2,256]{2,1,0:T(2,128)S(1)}, f32[16,2,128,256]{3,2,1,0:T(8,128)}) fusion(f32[16,2,128]{2,1,0:T(2,128)S(1)} %mul.188, f32[16,2,256]{2,1,0:T(2,128)S(1)} %mul.195, f32[16,2,128]{2,1,0:T(2,128)S(1)} %mul.193, f32[16,2,128,256]{3,2,1,0:T(8,128)} %param.18, f32[16,2,128]{2,1,0:T(2,128)S(1)} %mul.190), kind=kLoop, calls=%fused_computation | loop fusion | flops 5234688 | bytes 8503296 | tf_op jit(solution)/shard_map/reduce_sum | solution.py:53
  18.4 0.1 multiply_reduce_fusion.3
  18.6 0.1 broadcast_multiply_fusion
  18.7 3.0 %convolution_convert_fusion.2 = bf16[16,2048]{1,0:T(8,128)(2,1)} fusion(bf16[512,2048]{1,0:T(8,128)(2,1)S(1)} %copy-done, f32[16,512]{1,0:T(8,128)S(1)} %bitcast.96, f32[512]{0:T(512)S(1)} %bitcast.102, bf16[16,2048]{1,0:T(8,128)(2,1)S(1)} %copy-done.1, bf16[2048,512]{1,0:T(8,128)(2,1)} %param.23), kind=kOutput, calls=%fused_computation.5 | convolution fusion | flops 67198976 | bytes 4360192 | tf_op jit(solution)/shard_map/dot_general | solution.py:59
  21.7 0.0 all-reduce.3.cloned.1.call-update
  21.8 0.1 copy.52
  21.9 0.6 fusion.34
  22.4 0.1 eq.98
  22.5 0.1 fusion.27
  22.6 0.1 reduce_window_sum.11
  22.7 0.2 select_reduce_fusion
  22.9 0.1 reduce_sum.118
  23.0 0.8 fusion.10
  23.8 1.1 %reshape.146 = f32[16,2,32]{2,1,0:T(2,128)S(1)} reshape(f32[32,16,1,2]{3,1,0,2:T(8,128)} %fusion.10) | data formatting | bytes 8192 | tf_op jit(solution)/shard_map/rks,rd->sd/convert_element_type | solution.py:99
  24.9 0.1 copy.53
  25.0 0.6 multiply_add_fusion.3
  25.6 16.7 %all-reduce.3.cloned.1.call-done = bf16[16,2048]{1,0:T(8,128)(2,1)} async-done(((bf16[16,2048]{1,0:T(8,128)(2,1)}), bf16[16,2048]{1,0:T(8,128)(2,1)}) %all-reduce.3.cloned.1.call-update) | async-done | bytes 65552 | tf_op jit(solution)/shard_map/psum | solution.py:60
  42.4 1.0 %fusion.17 = f32[16]{0:T(128)S(1)} fusion(bf16[16,2048]{1,0:T(8,128)(2,1)} %all-reduce.3.cloned.1.call-done, bf16[16,2048]{1,0:T(8,128)(2,1)S(1)} %copy-done.1), kind=kLoop, calls=%fused_computation.27 | loop fusion | flops 163824 | bytes 131136 | tf_op jit(solution)/shard_map/reduce_sum | solution.py:11
  43.3 1.0 %multiply_reduce_fusion.1 = f32[16]{0:T(128)S(1)} fusion(bf16[16,2048]{1,0:T(8,128)(2,1)} %all-reduce.3.cloned.1.call-done, bf16[16,2048]{1,0:T(8,128)(2,1)S(1)} %copy-done.1, f32[16]{0:T(128)S(1)} %broadcast_multiply_fusion.2), kind=kLoop, calls=%fused_computation.23 | loop fusion | flops 229360 | bytes 131200 | tf_op jit(solution)/shard_map/reduce_sum | solution.py:12
  44.4 0.9 add_convert_fusion
  45.3 0.2 fusion.44
  45.5 0.7 reshape.139
  46.3 6.8 %all-to-all-start = ((bf16[16,1,2,2048]{3,2,1,0:T(2,128)(2,1)}), bf16[16,1,2,2048]{3,2,1,0:T(2,128)(2,1)S(1)}, u32[]{:S(2)}, u32[]{:S(2)}) async-start(bf16[16,1,2,2048]{3,2,1,0:T(2,128)(2,1)} %bitcast.4), calls=%async_computation | async-start | bytes 262144 | tf_op jit(solution)/shard_map/all_to_all | solution.py:108
  53.1 0.9 select_reduce_fusion.2
  54.0 0.1 fusion.43
  54.2 6.8 %all-to-all-done = bf16[16,1,2,2048]{3,2,1,0:T(2,128)(2,1)S(1)} async-done(((bf16[16,1,2,2048]{3,2,1,0:T(2,128)(2,1)}), bf16[16,1,2,2048]{3,2,1,0:T(2,128)(2,1)S(1)}, u32[]{:S(2)}, u32[]{:S(2)}) %all-to-all-start) | async-done | bytes 131104 | tf_op jit(solution)/shard_map/all_to_all | solution.py:108
  61.0 1.5 %convolution_bitcast_fusion.1 = f32[16,1,2,256]{3,0,2,1:T(8,128)S(1)} fusion(bf16[1,2048,256]{2,1,0:T(8,128)(2,1)} %param.31, bf16[16,1,2,2048]{3,2,1,0:T(2,128)(2,1)S(1)} %all-to-all-done), kind=kOutput, calls=%fused_computation.10 | convolution fusion | flops 33554432 | bytes 1212416 | tf_op jit(solution)/shard_map/secd,edf->secf/dot_general | solution.py:109
  62.5 2.0 %fusion = bf16[16,1,2,2048]{3,0,2,1:T(8,128)(2,1)S(1)} fusion(bf16[1,256,2048]{2,1,0:T(8,128)(2,1)S(1)} %copy-done.2, bf16[1,2048,256]{2,1,0:T(8,128)(2,1)} %param.32, bf16[16,1,2,2048]{3,2,1,0:T(2,128)(2,1)S(1)} %all-to-all-done, f32[16,1,2,256]{3,0,2,1:T(8,128)S(1)} %convolution_bitcast_fusion.1), kind=kOutput, calls=%fused_computation.4 | convolution fusion | flops 67223552 | bytes 2392064 | tf_op jit(solution)/shard_map/secf,efd->secd/dot_general | solution.py:114
  64.4 0.8 copy.56
  65.2 3.5 %all-to-all-start.1 = ((bf16[16,1,2,2048]{3,2,1,0:T(2,128)(2,1)}), bf16[16,1,2,2048]{3,2,1,0:T(2,128)(2,1)S(1)}, u32[]{:S(2)}, u32[]{:S(2)}) async-start(bf16[16,1,2,2048]{3,2,1,0:T(2,128)(2,1)} %copy.56), calls=%async_computation.1 | async-start | bytes 262144 | tf_op jit(solution)/shard_map/all_to_all | solution.py:118
  68.8 0.2 select_reduce_fusion.1
  69.0 7.6 %all-to-all-done.1 = bf16[16,1,2,2048]{3,2,1,0:T(2,128)(2,1)S(1)} async-done(((bf16[16,1,2,2048]{3,2,1,0:T(2,128)(2,1)}), bf16[16,1,2,2048]{3,2,1,0:T(2,128)(2,1)S(1)}, u32[]{:S(2)}, u32[]{:S(2)}) %all-to-all-start.1) | async-done | bytes 131104 | tf_op jit(solution)/shard_map/all_to_all | solution.py:118
  76.5 0.8 copy.57
  77.3 1.1 %reshape.152 = bf16[2,2,16384]{2,1,0:T(2,128)(2,1)S(1)} reshape(bf16[2048,1,2,16]{3,2,1,0:T(2,128)(2,1)S(1)} %bitcast.93) | data formatting | bytes 262144
  78.4 3.8 %all_to_all.25 = bf16[2,2,16384]{2,1,0:T(2,128)(2,1)S(1)} all-to-all(bf16[2,2,16384]{2,1,0:T(2,128)(2,1)S(1)} %reshape.152), channel_id=1, replica_groups=mesh['ep'=16,'tp'=2] {'tp'}, dimensions={0} | all-to-all | bytes 262144 | tf_op jit(solution)/shard_map/all_to_all | solution.py:117
  82.2 0.7 reshape.153
  82.9 0.8 copy.58
  83.7 0.1 reshape.150
  83.7 0.2 fusion.1
  84.0 0.1 fusion.32
  84.1 2.5 %all-reduce = (f32[16]{0:T(128)S(1)}, f32[16]{0:T(128)S(1)}) all-reduce(f32[16]{0:T(128)S(1)} %get-tuple-element.3, f32[16]{0:T(128)S(1)} %get-tuple-element.2), channel_id=1, replica_groups=mesh['ep'=16,'tp'=2] {'tp'}, use_global_device_ids=true, to_apply=%region_15.16 | all-reduce | flops 32 | bytes 256 | tf_op jit(solution)/shard_map/psum | solution.py:132
  86.6 0.7 add_convert_fusion.1
  (41 shorter events, 0.3 us)
Async XLA Ops:
  7.2 11.5 %copy-start = (bf16[512,2048]{1,0:T(8,128)(2,1)S(1)}, bf16[512,2048]{1,0:T(8,128)(2,1)}, u32[]{:S(2)}) copy-start(bf16[512,2048]{1,0:T(8,128)(2,1)} %param.25) | copy-start | bytes 6291460
  7.2 3.8 %copy-start.1 = (bf16[16,2048]{1,0:T(8,128)(2,1)S(1)}, bf16[16,2048]{1,0:T(8,128)(2,1)}, u32[]{:S(2)}) copy-start(bf16[16,2048]{1,0:T(8,128)(2,1)} %param.17) | copy-start | bytes 196612
  7.2 3.8 %copy-start.3 = (bf16[2048,256]{1,0:T(8,128)(2,1)S(1)}, bf16[2048,256]{1,0:T(8,128)(2,1)}, u32[]{:S(2)}) copy-start(bf16[2048,256]{1,0:T(8,128)(2,1)} %param.20) | copy-start | bytes 3145732
  7.2 35.2 %all-reduce.3.cloned.1.call-start = ((), (), s32[]{:S(2)}) async-start(), calls=%async_computation.3 | async-start | bytes 131072 | tf_op jit(solution)/shard_map/psum | solution.py:60
  12.8 5.9 %copy-start.9 = (f32[256]{0:T(256)S(1)}, f32[256]{0:T(256)}, u32[]{:S(2)}) copy-start(f32[256]{0:T(256)} %param.24) | copy-start | bytes 3076
  18.7 3.1 %copy-start.7 = (s32[16,2]{0,1:T(2,128)S(1)}, s32[16,2]{0,1:T(2,128)}, u32[]{:S(2)}) copy-start(s32[16,2]{0,1:T(2,128)} %param.30) | copy-start | bytes 388
  18.7 4.2 %copy-start.5 = (f32[2,2048]{1,0:T(2,128)S(1)}, f32[2,2048]{1,0:T(2,128)}, u32[]{:S(2)}) copy-start(f32[2,2048]{1,0:T(2,128)} %param.27) | copy-start | bytes 49156
  18.7 4.3 %copy-start.6 = (f32[2,2048]{1,0:T(2,128)S(1)}, f32[2,2048]{1,0:T(2,128)}, u32[]{:S(2)}) copy-start(f32[2,2048]{1,0:T(2,128)} %param.26) | copy-start | bytes 49156
  21.7 32.3 %copy-start.4 = (bf16[2048,32]{0,1:T(8,128)(2,1)S(1)}, bf16[2048,32]{0,1:T(8,128)(2,1)}, u32[]{:S(2)}) copy-start(bf16[2048,32]{0,1:T(8,128)(2,1)} %param.29) | copy-start | bytes 393220
  21.7 40.8 %copy-start.2 = (bf16[1,256,2048]{2,1,0:T(8,128)(2,1)S(1)}, bf16[1,256,2048]{2,1,0:T(8,128)(2,1)}, u32[]{:S(2)}) copy-start(bf16[1,256,2048]{2,1,0:T(8,128)(2,1)} %param.33) | copy-start | bytes 3145732
  46.3 14.7 %all-to-all-start = ((bf16[16,1,2,2048]{3,2,1,0:T(2,128)(2,1)}), bf16[16,1,2,2048]{3,2,1,0:T(2,128)(2,1)S(1)}, u32[]{:S(2)}, u32[]{:S(2)}) async-start(bf16[16,1,2,2048]{3,2,1,0:T(2,128)(2,1)} %bitcast.4), calls=%async_computation | async-start | bytes 262144 | tf_op jit(solution)/shard_map/all_to_all | solution.py:108
  65.2 11.3 %all-to-all-start.1 = ((bf16[16,1,2,2048]{3,2,1,0:T(2,128)(2,1)}), bf16[16,1,2,2048]{3,2,1,0:T(2,128)(2,1)S(1)}, u32[]{:S(2)}, u32[]{:S(2)}) async-start(bf16[16,1,2,2048]{3,2,1,0:T(2,128)(2,1)} %copy.56), calls=%async_computation.1 | async-start | bytes 262144 | tf_op jit(solution)/shard_map/all_to_all | solution.py:118
  77.3 6.5 %copy-start.8 = (s32[16,2]{0,1:T(2,128)S(1)}, s32[16,2]{0,1:T(2,128)}, u32[]{:S(2)}) copy-start(s32[16,2]{0,1:T(2,128)} %multiply_add_fusion.3) | copy-start | bytes 388
Sparse Core Ops, SparseCore 0:
  21.9 20.4 all-reduce.2
where the time goes:
time: 94.9 us; the launch traced here: 94.1 us
  waiting for transfers between devices  31.1 us (33%)
  between operations  14.4 us (15%)
  matrix products  13.3 us (14%)
  other arithmetic  12.1 us (13%)
  starting transfers between devices  10.4 us (11%)
  local copies, waits for them, and re-layouts  6.53 us (7%)
  blocking collectives  6.31 us (7%)
    psum x1, waiting for transfers between devices, on_device(): lax.psum(partial_value.astype(jnp.bfloat16), 'tp').astype(jnp.float32)  16.7 us
    all_to_all x1, waiting for transfers between devices, on_device(): lax.all_to_all(results, 'ep', split_axis=0, concat_axis=0, tiled=True)  7.57 us
    all_to_all x1, starting transfers between devices, on_device(): lax.all_to_all(outgoing, 'ep', split_axis=0, concat_axis=0, tiled=True)  6.83 us
    all_to_all x1, waiting for transfers between devices, on_device(): lax.all_to_all(outgoing, 'ep', split_axis=0, concat_axis=0, tiled=True)  6.8 us
    reduce_sum x1, other arithmetic, on_device(): readout = jnp.sum(queries[..., None] * new_state, axis=2)  5.65 us
    dot_general x4, matrix products, project(): return jnp.dot(tokens, weight, preferred_element_type=jnp.float32)  5.4 us
    all_to_all x1, blocking collectives, on_device(): lax.all_to_all(lax.all_to_all(results, 'ep', split_axis=0, concat_axis=0,...  3.84 us
    all_to_all x1, starting transfers between devices, on_device(): lax.all_to_all(results, 'ep', split_axis=0, concat_axis=0, tiled=True)  3.51 us
  transfers between devices with their start and end apart: 3, of which 3 were waited for; matrix products, arithmetic and copies ran while one was open for 5% of the time, Pallas kernels for 0%

commit v1 on v0

--- a/solution.py
+++ b/solution.py
@@ -11,6 +11,11 @@
     centered = inputs - jnp.mean(inputs, axis=-1, keepdims=True)
     spread = jnp.mean(centered * centered, axis=-1, keepdims=True)
     return centered * lax.rsqrt(spread + eps_norm) * gain_row + bias_row
+
+
+def swapped(values):
+    count = lax.axis_size("tp")
+    return lax.ppermute(values, "tp", [(i, (i + 1) % count) for i in range(count)])
 
 
 def on_device(
@@ -47,17 +52,18 @@
     decay_rate = jnp.exp(jax.nn.log_sigmoid(project(decay_weight)) / 16.0).reshape(
         row_count, heads_here, key_dim
     )
-    new_state = (
-        decay_rate[..., None] * recurrent_state + key_rows[..., None] * value_rows[:, :, None, :]
+    readout = (
+        jnp.sum((queries * decay_rate)[..., None] * recurrent_state, axis=2)
+        + jnp.sum(queries * key_rows, axis=-1, keepdims=True) * value_rows
     )
-    readout = jnp.sum(queries[..., None] * new_state, axis=2)
     norm_scale = lax.rsqrt(jnp.mean(readout * readout, axis=-1, keepdims=True) + eps_norm)
     gated_rows = (
         (readout * norm_scale * head_gain).reshape(row_count, heads_here * value_dim)
         * jax.nn.silu(gate_rows)
     ).astype(jnp.bfloat16)
     partial_value = jnp.dot(gated_rows, output_weight, preferred_element_type=jnp.float32)
-    mixed_sum = lax.psum(partial_value.astype(jnp.bfloat16), "tp").astype(jnp.float32)
+    own_part = partial_value.astype(jnp.bfloat16)
+    mixed_sum = own_part.astype(jnp.float32) + swapped(own_part).astype(jnp.float32)
     hidden = layer_normed(
         alpha_res * tokens.astype(jnp.float32) + mixed_sum, norm_gain[0], norm_bias[0]
     ).astype(jnp.bfloat16)
@@ -105,7 +111,14 @@
     outgoing = outgoing.reshape(ep_count, local_experts, capacity, model_width)
     col_width = model_width // tp_count
     col_start = pair_index * col_width
+    late_decay, late_keys, late_values, outgoing = lax.optimization_barrier(
+        (decay_rate, key_rows, value_rows, outgoing)
+    )
+    new_state = (
+        late_decay[..., None] * recurrent_state + late_keys[..., None] * late_values[:, :, None, :]
+    )
     arrived = lax.all_to_all(outgoing, "ep", split_axis=0, concat_axis=0, tiled=True)
+    arrived, new_state = lax.optimization_barrier((arrived, new_state))
     gate_part = jnp.einsum(
         "secd,edf->secf", arrived, expert_gate, preferred_element_type=jnp.float32
     )
@@ -114,13 +127,10 @@
     results = jnp.einsum(
         "secf,efd->secd", activation, expert_down, preferred_element_type=jnp.float32
     ).astype(jnp.bfloat16)
-    returned = lax.all_to_all(
-        lax.all_to_all(results, "ep", split_axis=0, concat_axis=0, tiled=True),
-        "tp",
-        split_axis=3,
-        concat_axis=1,
-        tiled=True,
-    )
+    halves = jnp.transpose(
+        results.reshape(ep_count, local_experts * capacity, tp_count, col_width), (0, 2, 1, 3)
+    ).reshape(ep_count * tp_count, local_experts * capacity, col_width)
+    returned = lax.all_to_all(halves, ("ep", "tp"), split_axis=0, concat_axis=0, tiled=True)
     fetched = jnp.dot(
         pick_all, returned.reshape(total_slots, col_width), preferred_element_type=jnp.float32
     ).reshape(row_count, top_count, col_width)
@@ -129,9 +139,8 @@
         alpha_res * lax.dynamic_slice_in_dim(hidden, col_start, col_width, 1).astype(jnp.float32)
         + routed_sum
     )
-    row_total, row_squares = lax.psum(
-        (jnp.sum(blended, axis=1), jnp.sum(blended * blended, axis=1)), "tp"
-    )
+    own_stats = jnp.stack((jnp.sum(blended, axis=1), jnp.sum(blended * blended, axis=1)))
+    row_total, row_squares = own_stats + swapped(own_stats)
     row_mean = row_total / model_width
     spread = row_squares / model_width - row_mean * row_mean
     gain_part = lax.dynamic_slice_in_dim(norm_gain[1], col_start, col_width, 0)

time: 94.9 us -> 49.9 us (0.53)
  waiting for transfers between devices: 31.1 us -> 12.4 us
  between operations: 14.4 us -> 1.04 us
  blocking collectives: 6.31 us -> 0 us
  local copies, waits for them, and re-layouts: 6.53 us -> 2.54 us
  other arithmetic: 12.1 us -> 9.76 us
    psum x1 -> x0, waiting for transfers between devices: 16.7 us -> none  [on_device(): lax.psum(partial_value.astype(jnp.bfloat16), 'tp').astype(jnp.float32)]
    add x0 -> x2, other arithmetic: none -> 4.32 us  [the longest x1 4.31 us: on_device(): late_decay[..., None] * recurrent_state]
    all_to_all x1 -> x0, blocking collectives: 3.84 us -> none  [on_device(): lax.all_to_all(lax.all_to_all(results, 'ep', split_axis=0, concat_axis=0,...]
    all_to_all x1, waiting for transfers between devices: 6.8 us -> 3.41 us  [on_device(): lax.all_to_all(outgoing, 'ep', split_axis=0, concat_axis=0, tiled=True)]
    reduce_sum x1 -> x2, other arithmetic: 5.65 us -> 2.72 us  [the longest x1 2.62 us: on_device(): jnp.sum((queries * decay_rate)[..., None] * recurrent_state, axis=2)]
    psum x1 -> x0, blocking collectives: 2.47 us -> none  [on_device(): lax.psum((jnp.sum(blended, axis=1), jnp.sum(blended * blended, axis=1)),...]
    unnamed x26 -> x28, local copies, waits for them, and re-layouts: 1.93 us -> 0.17 us
    all_to_all x2 -> x0, local copies, waits for them, and re-layouts: 1.51 us -> none  [the longest x1 0.76 us: on_device(): lax.all_to_all(results, 'ep', split_axis=0, concat_axis=0, tiled=True)]
  transfers between devices with their start and end apart: 3 -> 4, of which waited for: 3 -> 3; matrix products, arithmetic and copies ran while one was open for 5% -> 13% of each run, Pallas kernels for 0% -> 0%
where the time goes in v1:
time: 49.9 us; the launch traced here: 49.5 us
  matrix products  12.6 us (25%)
  waiting for transfers between devices  12.4 us (25%)
  starting transfers between devices  11.2 us (22%)
  other arithmetic  9.76 us (20%)
  local copies, waits for them, and re-layouts  2.54 us (5%)
  between operations  1.04 us (2%)
    all_to_all x1, waiting for transfers between devices, on_device(): lax.all_to_all(halves, ('ep', 'tp'), split_axis=0, concat_axis=0, tiled=T...  7.99 us
    all_to_all x1, starting transfers between devices, on_device(): lax.all_to_all(outgoing, 'ep', split_axis=0, concat_axis=0, tiled=True)  7.88 us
    dot_general x4, matrix products, project(): return jnp.dot(tokens, weight, preferred_element_type=jnp.float32)  5.4 us
    add x1, other arithmetic, on_device(): late_decay[..., None] * recurrent_state  4.31 us
    all_to_all x1, waiting for transfers between devices, on_device(): lax.all_to_all(outgoing, 'ep', split_axis=0, concat_axis=0, tiled=True)  3.41 us
    reduce_sum x1, other arithmetic, on_device(): jnp.sum((queries * decay_rate)[..., None] * recurrent_state, axis=2)  2.62 us
    all_to_all x1, starting transfers between devices, on_device(): lax.all_to_all(halves, ('ep', 'tp'), split_axis=0, concat_axis=0, tiled=T...  2.57 us
    dot_general x1, matrix products, on_device(): jnp.dot(gated_rows, output_weight, preferred_element_type=jnp.float32)  2.35 us
  transfers between devices with their start and end apart: 4, of which 3 were waited for; matrix products, arithmetic and copies ran while one was open for 13% of the time, Pallas kernels for 0%

profile of v1, /device:TPU:0, one launch (start us, length us, event | category | flops | bytes accessed | tf_op | source)
XLA Modules:
  0.0 49.5 jit_solution(17508484035689143754)
XLA Ops:
  0.6 0.0 copy-start
  0.6 0.0 copy-start.1
  0.7 1.7 %fusion.22 = f32[16,256]{1,0:T(8,128)S(1)} fusion(bf16[16,2048]{1,0:T(8,128)(2,1)} %param.17, bf16[2048,256]{1,0:T(8,128)(2,1)} %param.21), kind=kOutput, calls=%fused_computation.39 | convolution fusion | flops 16814080 | bytes 1130496 | tf_op jit(solution)/shard_map/dot_general | solution.py:46
  2.4 1.5 %fusion.41 = f32[16,256]{1,0:T(8,128)S(1)} fusion(bf16[16,2048]{1,0:T(8,128)(2,1)} %param.17, bf16[2048,256]{1,0:T(8,128)(2,1)} %param.20), kind=kOutput, calls=%fused_computation.84 | convolution fusion | flops 16777216 | bytes 1130496 | tf_op jit(solution)/shard_map/dot_general | solution.py:46
  3.9 2.0 %fusion.42 = f32[16,512]{1,0:T(8,128)S(1)} fusion(bf16[16,2048]{1,0:T(8,128)(2,1)S(1)} %copy-done.1, bf16[2048,512]{1,0:T(8,128)(2,1)} %param.22), kind=kOutput, calls=%fused_computation.85 | convolution fusion | flops 33554432 | bytes 2195456 | tf_op jit(solution)/shard_map/dot_general | solution.py:46
  5.9 0.2 convolution_multiply_fusion.1
  6.2 0.1 multiply_reduce_fusion.4
  6.3 2.6 %multiply_reduce_fusion = f32[16,2,256]{2,1,0:T(2,128)S(1)} fusion(f32[16,2,128,256]{3,2,1,0:T(8,128)} %param.18, f32[16,2,128]{2,1,0:T(2,128)S(1)} %get-tuple-element.17), kind=kLoop, calls=%fused_computation.1 | loop fusion | flops 2088960 | bytes 4243456 | tf_op jit(solution)/shard_map/reduce_sum | solution.py:56
  8.9 0.2 multiply_reduce_fusion.3
  9.1 0.1 mul.218
  9.2 0.1 mul.213
  9.4 0.0 copy-start.7
  9.4 2.4 %convolution_convert_fusion.2 = bf16[16,2048]{1,0:T(8,128)(2,1)S(1)} fusion(bf16[512,2048]{1,0:T(8,128)(2,1)S(1)} %copy-done, f32[16,512]{1,0:T(8,128)S(1)} %bitcast.108, f32[16,512]{1,0:T(8,128)S(1)} %bitcast.109, f32[16,512]{1,0:T(8,128)S(1)} %bitcast.110, f32[16,512]{1,0:T(8,128)S(1)} %fusion.42, f32[512]{0:T(512)S(1)} %bitcast.117, ...), kind=kOutput, calls=%fused_computation.5 | convolution fusion | flops 67223552 | bytes 4458496 | tf_op jit(solution)/shard_map/dot_general | solution.py:64
  11.8 0.5 %collective-permute-start = (bf16[16,2048]{1,0:T(8,128)(2,1)S(1)}, bf16[16,2048]{1,0:T(8,128)(2,1)S(1)}, u32[]{:S(2)}, u32[]{:S(2)}) collective-permute-start(bf16[16,2048]{1,0:T(8,128)(2,1)S(1)} %convolution_convert_fusion.2), channel_id=1, source_target_pairs={{0,1},{1,0},{2,3},{3,2},{4,5},{5,4},{6,7},{7,6},{8,9},{9,8},{10,11... | collective-permute-start | bytes 196616 | tf_op jit(solution)/shard_map/ppermute | solution.py:18
  12.3 0.1 copy.50
  12.4 0.1 eq.98
  12.5 0.1 fusion.24
  12.5 0.1 reduce_window_sum.11
  12.6 0.2 select_reduce_fusion
  12.8 0.1 reduce_sum.131
  12.9 0.0 copy-done.5
  12.9 0.1 copy.51
  13.0 0.6 %multiply_add_fusion.3 = s32[16,2]{0,1:T(2,128)} fusion(s32[16,2]{0,1:T(2,128)S(1)} %copy.51, s32[16,2]{0,1:T(2,128)S(1)} %copy-done.7), kind=kLoop, calls=%fused_computation.63 | loop fusion | flops 64 | bytes 384 | tf_op jit(solution)/shard_map/add | solution.py:95
  13.6 0.1 fusion.10
  13.7 0.2 reshape.190
  13.9 0.1 fusion.19
  14.1 0.2 multiply_reduce_fusion.1
  14.3 0.1 add_convert_fusion
  14.4 0.2 fusion.44
  14.6 0.7 %reshape.181 = bf16[16,1,2,2048]{3,2,0,1:T(2,128)(2,1)} reshape(bf16[32,2048]{1,0:T(8,128)(2,1)S(1)} %fusion.44) | data formatting | bytes 262144 | tf_op jit(solution)/shard_map/reshape | solution.py:111
  15.4 7.9 %all-to-all-start = ((bf16[16,1,2,2048]{3,2,1,0:T(2,128)(2,1)}), bf16[16,1,2,2048]{3,2,1,0:T(2,128)(2,1)S(1)}, u32[]{:S(2)}, u32[]{:S(2)}) async-start(bf16[16,1,2,2048]{3,2,1,0:T(2,128)(2,1)} %bitcast.4), calls=%async_computation | async-start | bytes 262144 | tf_op jit(solution)/shard_map/all_to_all | solution.py:120
  23.3 0.1 select_reduce_fusion.2
  23.5 4.3 %multiply_add_fusion = f32[16,2,128,256]{3,2,1,0:T(8,128)} fusion(f32[16,2,128,256]{3,2,1,0:T(8,128)} %param.18, f32[16,2,256]{2,1,0:T(2,128)S(1)} %reshape.180, f32[16,2,128]{2,1,0:T(2,128)S(1)} %reshape.179, f32[16,2,128]{2,1,0:T(2,128)S(1)} %reshape.178), kind=kLoop, calls=%fused_computation | loop fusion | flops 3145728 | bytes 8454144 | tf_op jit(solution)/shard_map/add | solution.py:118
  27.8 0.1 fusion.43
  27.9 3.4 %all-to-all-done = bf16[16,1,2,2048]{3,2,1,0:T(2,128)(2,1)S(1)} async-done(((bf16[16,1,2,2048]{3,2,1,0:T(2,128)(2,1)}), bf16[16,1,2,2048]{3,2,1,0:T(2,128)(2,1)S(1)}, u32[]{:S(2)}, u32[]{:S(2)}) %all-to-all-start) | async-done | bytes 131104 | tf_op jit(solution)/shard_map/all_to_all | solution.py:120
  31.3 1.5 %convolution_bitcast_fusion.1 = f32[16,1,2,256]{3,0,2,1:T(8,128)S(1)} fusion(bf16[1,2048,256]{2,1,0:T(8,128)(2,1)} %param.31, bf16[16,2,2048]{2,1,0:T(2,128)(2,1)S(1)} %bitcast.104), kind=kOutput, calls=%fused_computation.10 | convolution fusion | flops 33554432 | bytes 1212416 | tf_op jit(solution)/shard_map/secd,edf->secf/dot_general | solution.py:122
  32.9 2.0 %fusion = bf16[16,1,2,2048]{3,0,2,1:T(8,128)(2,1)S(1)} fusion(bf16[1,256,2048]{2,1,0:T(8,128)(2,1)S(1)} %copy-done.2, bf16[1,2048,256]{2,1,0:T(8,128)(2,1)} %param.32, bf16[16,2,2048]{2,1,0:T(2,128)(2,1)S(1)} %bitcast.105, f32[16,1,2,256]{3,0,2,1:T(8,128)S(1)} %convolution_bitcast_fusion.1), kind=kOutput, calls=%fused_computation.4 | convolution fusion | flops 67223552 | bytes 2392064 | tf_op jit(solution)/shard_map/secf,efd->secd/dot_general | solution.py:127
  34.8 0.1 reshape.187
  34.9 0.8 %copy.56 = bf16[16,2,2,1024]{3,2,1,0:T(2,128)(2,1)} copy(bf16[16,2,2,1024]{3,1,0,2:T(2,128)(2,1)S(1)} %bitcast.106) | data formatting | bytes 262144 | tf_op jit(solution)/shard_map/reshape | solution.py:132
  35.7 2.6 %all-to-all-start.1 = ((bf16[32,2,1024]{2,1,0:T(2,128)(2,1)}), bf16[32,2,1024]{2,1,0:T(2,128)(2,1)S(1)}, u32[]{:S(2)}, u32[]{:S(2)}) async-start(bf16[32,2,1024]{2,1,0:T(2,128)(2,1)} %bitcast.25), calls=%async_computation.1 | async-start | bytes 262144 | tf_op jit(solution)/shard_map/all_to_all | solution.py:133
  38.3 0.2 select_reduce_fusion.1
  38.5 8.0 %all-to-all-done.1 = bf16[32,2,1024]{2,1,0:T(2,128)(2,1)S(1)} async-done(((bf16[32,2,1024]{2,1,0:T(2,128)(2,1)}), bf16[32,2,1024]{2,1,0:T(2,128)(2,1)S(1)}, u32[]{:S(2)}, u32[]{:S(2)}) %all-to-all-start.1) | async-done | bytes 131104 | tf_op jit(solution)/shard_map/all_to_all | solution.py:133
  46.5 0.1 reshape.194
  46.5 0.9 %fusion.1 = f32[16,1024]{1,0:T(8,128)S(1)} fusion(bf16[64,1024,1]{1,0,2:T(8,128)(2,1)S(1)} %reshape.194, f32[16,2]{0,1:T(2,128)S(1)} %divide_multiply_fusion, s32[16,2]{0,1:T(2,128)} %multiply_add_fusion.3), kind=kOutput, calls=%fused_computation.7 | convolution fusion | flops 4245504 | bytes 196864 | tf_op jit(solution)/shard_map/dot_general | solution.py:134
  47.4 0.1 fusion.29
  47.6 0.3 collective-permute-start.1
  47.9 0.9 %collective-permute-done.1 = f32[2,16]{1,0:T(2,128)S(1)} collective-permute-done((f32[2,16]{1,0:T(2,128)S(1)}, f32[2,16]{1,0:T(2,128)S(1)}, u32[]{:S(2)}, u32[]{:S(2)}) %collective-permute-start.1) | collective-permute-done | bytes 160 | tf_op jit(solution)/shard_map/ppermute | solution.py:18
  48.8 0.7 %add_convert_fusion.1 = bf16[16,1024]{1,0:T(8,128)(2,1)} fusion(f32[1024]{0:T(1024)S(1)} %bitcast.115, f32[1024]{0:T(1024)S(1)} %bitcast.116, f32[16]{0:T(128)S(1)} %fusion.32, f32[16]{0:T(128)S(1)} %multiply_bitcast_fusion, f32[16,1024]{1,0:T(8,128)S(1)} %fusion.1, bf16[16,2048]{1,0:T(8,128)(2,1)S(1)} %add_convert_fusion, s32[]{:T(128)S(6)} %select_n.28), kind=kLoop, calls=%fused_computation.25 | loop fusion | flops 131072 | bytes 139396 | tf_op jit(solution)/shard_map/convert_element_type | solution.py:151
  (47 shorter events, 0.4 us)
Async XLA Ops:
  0.6 8.7 %copy-start = (bf16[512,2048]{1,0:T(8,128)(2,1)S(1)}, bf16[512,2048]{1,0:T(8,128)(2,1)}, u32[]{:S(2)}) copy-start(bf16[512,2048]{1,0:T(8,128)(2,1)} %param.25) | copy-start | bytes 6291460
  0.6 3.3 %copy-start.1 = (bf16[16,2048]{1,0:T(8,128)(2,1)S(1)}, bf16[16,2048]{1,0:T(8,128)(2,1)}, u32[]{:S(2)}) copy-start(bf16[16,2048]{1,0:T(8,128)(2,1)} %param.17) | copy-start | bytes 196612
  0.7 5.3 %copy-start.3 = (bf16[2048,256]{1,0:T(8,128)(2,1)S(1)}, bf16[2048,256]{1,0:T(8,128)(2,1)}, u32[]{:S(2)}) copy-start(bf16[2048,256]{1,0:T(8,128)(2,1)} %param.19) | copy-start | bytes 3145732
  6.3 3.0 %copy-start.9 = (f32[256]{0:T(256)S(1)}, f32[256]{0:T(256)}, u32[]{:S(2)}) copy-start(f32[256]{0:T(256)} %param.24) | copy-start | bytes 3076
  9.4 2.9 %copy-start.7 = (s32[16,2]{0,1:T(2,128)S(1)}, s32[16,2]{0,1:T(2,128)}, u32[]{:S(2)}) copy-start(s32[16,2]{0,1:T(2,128)} %param.30) | copy-start | bytes 388
  9.4 3.5 %copy-start.5 = (f32[2,2048]{1,0:T(2,128)S(1)}, f32[2,2048]{1,0:T(2,128)}, u32[]{:S(2)}) copy-start(f32[2,2048]{1,0:T(2,128)} %param.27) | copy-start | bytes 49156
  9.4 3.5 %copy-start.6 = (f32[2,2048]{1,0:T(2,128)S(1)}, f32[2,2048]{1,0:T(2,128)}, u32[]{:S(2)}) copy-start(f32[2,2048]{1,0:T(2,128)} %param.26) | copy-start | bytes 49156
  11.8 11.5 %copy-start.10 = (bf16[2048,4]{0,1:T(4,128)(2,1)S(1)}, bf16[2048,4]{0,1:T(4,128)(2,1)}, u32[]{:S(2)}) copy-start(bf16[2048,4]{0,1:T(4,128)(2,1)} %param.28) | copy-start | bytes 49156
  11.8 2.2 %collective-permute-start = (bf16[16,2048]{1,0:T(8,128)(2,1)S(1)}, bf16[16,2048]{1,0:T(8,128)(2,1)S(1)}, u32[]{:S(2)}, u32[]{:S(2)}) collective-permute-start(bf16[16,2048]{1,0:T(8,128)(2,1)S(1)} %convolution_convert_fusion.2), channel_id=1, source_target_pairs={{0,1},{1,0},{2,3},{3,2},{4,5},{5,4},{6,7},{7,6},{8,9},{9,8},{10,11... | collective-permute-start | bytes 196616 | tf_op jit(solution)/shard_map/ppermute | solution.py:18
  15.4 16.0 %all-to-all-start = ((bf16[16,1,2,2048]{3,2,1,0:T(2,128)(2,1)}), bf16[16,1,2,2048]{3,2,1,0:T(2,128)(2,1)S(1)}, u32[]{:S(2)}, u32[]{:S(2)}) async-start(bf16[16,1,2,2048]{3,2,1,0:T(2,128)(2,1)} %bitcast.4), calls=%async_computation | async-start | bytes 262144 | tf_op jit(solution)/shard_map/all_to_all | solution.py:120
  23.4 4.3 %copy-start.4 = (bf16[2048,32]{0,1:T(8,128)(2,1)S(1)}, bf16[2048,32]{0,1:T(8,128)(2,1)}, u32[]{:S(2)}) copy-start(bf16[2048,32]{0,1:T(8,128)(2,1)} %param.29) | copy-start | bytes 393220
  23.4 9.4 %copy-start.2 = (bf16[1,256,2048]{2,1,0:T(8,128)(2,1)S(1)}, bf16[1,256,2048]{2,1,0:T(8,128)(2,1)}, u32[]{:S(2)}) copy-start(bf16[1,256,2048]{2,1,0:T(8,128)(2,1)} %param.33) | copy-start | bytes 3145732
  31.3 6.9 %copy-start.8 = (s32[16,2]{0,1:T(2,128)S(1)}, s32[16,2]{0,1:T(2,128)}, u32[]{:S(2)}) copy-start(s32[16,2]{0,1:T(2,128)} %param.30) | copy-start | bytes 388
  35.7 10.8 %all-to-all-start.1 = ((bf16[32,2,1024]{2,1,0:T(2,128)(2,1)}), bf16[32,2,1024]{2,1,0:T(2,128)(2,1)S(1)}, u32[]{:S(2)}, u32[]{:S(2)}) async-start(bf16[32,2,1024]{2,1,0:T(2,128)(2,1)} %bitcast.25), calls=%async_computation.1 | async-start | bytes 262144 | tf_op jit(solution)/shard_map/all_to_all | solution.py:133
  47.6 1.2 %collective-permute-start.1 = (f32[2,16]{1,0:T(2,128)S(1)}, f32[2,16]{1,0:T(2,128)S(1)}, u32[]{:S(2)}, u32[]{:S(2)}) collective-permute-start(f32[2,16]{1,0:T(2,128)S(1)} %pad_maximum_fusion), channel_id=1, source_target_pairs={{0,1},{1,0},{2,3},{3,2},{4,5},{5,4},{6,7},{7,6},{8,9},{9,8},{10,11... | collective-permute-start | bytes 392 | tf_op jit(solution)/shard_map/ppermute | solution.py:18

commit v2 on v1

v2 whole, which is shorter than its diff:
```python
import functools

import jax
import jax.numpy as jnp
from jax import lax
from jax.experimental import pallas as pl
from jax.experimental.pallas import tpu as pltpu
from jax.sharding import PartitionSpec as P

alpha_res = 2.0**0.5
eps_norm = 1e-05
mib = 1024 * 1024
cells = 8
in_vmem = pl.BlockSpec(memory_space=pltpu.VMEM)
in_hbm = pl.BlockSpec(memory_space=pltpu.HBM)
in_smem = pl.BlockSpec(memory_space=pltpu.SMEM)


def swapped(values):
    count = lax.axis_size("tp")
    return lax.ppermute(values, "tp", [(i, (i + 1) % count) for i in range(count)])


def dot32(left, right):
    return jnp.dot(left, right, preferred_element_type=jnp.float32)


def mix_kernel(
    key_dim, value_dim, tokens_ref, gain_ref, wq, wd, wk, wv, wg, state, wo,
    part_ref, key_ref, decay_ref, value_ref,
    q_buf, d_buf, k_buf, v_buf, g_buf, s_buf, o_buf, read_buf, sems,
):
    pairs = ((wq, q_buf), (wd, d_buf), (wk, k_buf), (state, s_buf), (wv, v_buf), (wg, g_buf), (wo, o_buf))
    copies = [pltpu.make_async_copy(a, b, sems.at[n]) for n, (a, b) in enumerate(pairs)]
    for copy in copies:
        copy.start()
    heads = q_buf.shape[1] // key_dim
    row_count = tokens_ref.shape[0]
    copies[0].wait()
    queries = dot32(tokens_ref[...], q_buf[...]) * key_dim ** (-0.5)
    copies[1].wait()
    raw = dot32(tokens_ref[...], d_buf[...])
    log_sig = jnp.minimum(raw, 0.0) - jnp.log(1.0 + jnp.exp(-jnp.abs(raw)))
    decay = jnp.exp(log_sig / 16.0)
    decay_ref[...] = decay
    copies[2].wait()
    keys = dot32(tokens_ref[...], k_buf[...])
    key_ref[...] = keys
    scaled = queries * decay
    copies[3].wait()
    for h in range(heads):
        cols = jnp.transpose(scaled[:, h * key_dim : (h + 1) * key_dim])
        for b in range(row_count):
            read_buf[h, b : b + 1, :] = jnp.sum(
                cols[:, b : b + 1] * s_buf[b, h], axis=0, keepdims=True
            )
    copies[4].wait()
    values = dot32(tokens_ref[...], v_buf[...])
    value_ref[...] = values
    copies[5].wait()
    gates = dot32(tokens_ref[...], g_buf[...])
    gates = gates * jax.nn.sigmoid(gates)
    gated = []
    for h in range(heads):
        ks = slice(h * key_dim, (h + 1) * key_dim)
        vs = slice(h * value_dim, (h + 1) * value_dim)
        readout = read_buf[h] + jnp.sum(queries[:, ks] * keys[:, ks], axis=1, keepdims=True) * values[:, vs]
        scale = lax.rsqrt(jnp.mean(readout * readout, axis=1, keepdims=True) + eps_norm)
        gated.append((readout * scale * gain_ref[...] * gates[:, vs]).astype(jnp.bfloat16))
    gated = jnp.concatenate(gated, axis=1)
    copies[6].wait()
    part_ref[...] = dot32(gated, o_buf[...]).astype(jnp.bfloat16)


def mix(tokens, state, wq, wk, wd, wv, wg, gain, wo):
    rows, heads, key_dim, value_dim = state.shape
    f32 = jnp.float32
    weights = (wq, wd, wk, wv, wg)
    return pl.pallas_call(
        functools.partial(mix_kernel, key_dim, value_dim),
        out_shape=(
            jax.ShapeDtypeStruct((rows, wo.shape[1]), jnp.bfloat16),
            jax.ShapeDtypeStruct((rows, wk.shape[1]), f32),
            jax.ShapeDtypeStruct((rows, wd.shape[1]), f32),
            jax.ShapeDtypeStruct((rows, wv.shape[1]), f32),
        ),
        in_specs=[in_vmem] * 2 + [in_hbm] * 7,
        out_specs=[in_vmem] * 4,
        scratch_shapes=[pltpu.VMEM(w.shape, w.dtype) for w in weights]
        + [
            pltpu.VMEM(state.shape, f32),
            pltpu.VMEM(wo.shape, wo.dtype),
            pltpu.VMEM((heads, rows, value_dim), f32),
            pltpu.SemaphoreType.DMA((7,)),
        ],
        compiler_params=pltpu.CompilerParams(vmem_limit_bytes=28 * mib),
        cost_estimate=pl.CostEstimate(flops=200_000_000, bytes_accessed=14 * mib, transcendentals=0),
    )(tokens, gain.reshape(1, -1), wq, wd, wk, wv, wg, state, wo)


def send_kernel(
    tp_count, pieces, pair_ref, own_ref, other_ref, tokens_ref, gain_ref, bias_ref, routes_ref, lanes_ref,
    hidden_ref, out_ref,
):
    mixed = own_ref[...].astype(jnp.float32) + other_ref[...].astype(jnp.float32)
    total = alpha_res * tokens_ref[...].astype(jnp.float32) + mixed
    centered = total - jnp.mean(total, axis=1, keepdims=True)
    spread = jnp.mean(centered * centered, axis=1, keepdims=True)
    hidden = (centered * lax.rsqrt(spread + eps_norm) * gain_ref[0:1, :] + bias_ref[0:1, :]).astype(jnp.bfloat16)
    hidden_ref[...] = hidden
    rows, width = hidden.shape
    span = width // pieces
    lanes = rows * pieces
    top = routes_ref.shape[1]
    cap = cells // pieces
    lane = lax.broadcasted_iota(jnp.int32, (rows, lanes), 1)
    earlier = lax.broadcasted_iota(jnp.int32, (rows, lanes), 0) < lax.rem(lane, rows)
    piece = lax.div(lax.broadcasted_iota(jnp.int32, (1, lanes), 1), rows)
    place = lax.broadcasted_iota(jnp.int32, (out_ref.shape[0], lanes), 0)
    pick = jnp.zeros((out_ref.shape[0], lanes), jnp.float32)
    for k in range(top):
        mine = lanes_ref[k : k + 1, :]
        count = jnp.zeros((1, lanes), jnp.int32)
        for j in range(top):
            same = (routes_ref[:, j : j + 1] == mine) & earlier
            count = count + jnp.sum(same.astype(jnp.int32), axis=0, keepdims=True)
        target = lax.div(mine, tp_count) * cells + count * pieces + piece
        target = jnp.where(lax.rem(mine, tp_count) == pair_ref[0], target, -1)
        pick = pick + (place == target).astype(jnp.float32)
    stack = jnp.concatenate([hidden[:, q * span : (q + 1) * span] for q in range(pieces)], axis=0)
    out_ref[...] = dot32(pick.astype(jnp.bfloat16), stack).astype(jnp.bfloat16)


def expert_kernel(tp_count, pieces, in_ref, gate_ref, up_ref, down_ref, out_ref):
    cap = cells // pieces
    span = in_ref.shape[1]
    total = in_ref.shape[0]
    batch = min(total, 16 * cells)
    sources = batch // cells
    rows = sources * cap
    width = down_ref.shape[2]
    slots = tp_count * pieces
    narrow = width // slots
    row = lax.broadcasted_iota(jnp.int32, (rows, batch), 0)
    col = lax.broadcasted_iota(jnp.int32, (rows, batch), 1)
    place = lax.broadcasted_iota(jnp.int32, (rows * slots, rows * slots), 0)
    origin = lax.broadcasted_iota(jnp.int32, (rows * slots, rows * slots), 1)
    dest = lax.div(place, cells)
    cell = lax.rem(place, cells)
    wanted = (
        (lax.rem(dest, tp_count) * pieces + lax.rem(cell, pieces)) * rows
        + lax.div(dest, tp_count) * cap
        + lax.div(cell, pieces)
    )
    order = (wanted == origin).astype(jnp.float32).astype(jnp.bfloat16)
    for n in range(total // batch):
        block = in_ref[n * batch : (n + 1) * batch, :]
        parts = [
            dot32((col == row * pieces + q).astype(jnp.float32).astype(jnp.bfloat16), block).astype(jnp.bfloat16)
            for q in range(pieces)
        ]
        wide = jnp.concatenate(parts, axis=1)
        gate = dot32(wide, gate_ref[0])
        up = dot32(wide, up_ref[0])
        active = (gate * jax.nn.sigmoid(gate) * up).astype(jnp.bfloat16)
        result = dot32(active, down_ref[0]).astype(jnp.bfloat16)
        stack = jnp.concatenate([result[:, j * narrow : (j + 1) * narrow] for j in range(slots)], axis=0)
        out_ref[n * rows * slots : (n + 1) * rows * slots, :] = dot32(order, stack).astype(jnp.bfloat16)


def blend_kernel(pieces, pair_ref, got_ref, routes_ref, lanes_ref, weight_ref, hidden_ref, blend_ref, stat_ref):
    rows, top = routes_ref.shape
    width = blend_ref.shape[1]
    narrow = got_ref.shape[1]
    cap = cells // pieces
    earlier = lax.broadcasted_iota(jnp.int32, (rows, rows), 1) < lax.broadcasted_iota(jnp.int32, (rows, rows), 0)
    place = lax.broadcasted_iota(jnp.int32, (rows, got_ref.shape[0]), 1)
    picks = []
    for k in range(top):
        mine = routes_ref[:, k : k + 1]
        count = jnp.zeros((rows, 1), jnp.int32)
        for j in range(top):
            same = (lanes_ref[j : j + 1, :rows] == mine) & earlier
            count = count + jnp.sum(same.astype(jnp.int32), axis=1, keepdims=True)
        for q in range(pieces):
            picks.append((place == mine * cells + count * pieces + q).astype(jnp.float32))
    chosen = dot32(jnp.concatenate(picks, axis=0).astype(jnp.bfloat16), got_ref[...])
    start = pl.multiple_of(pair_ref[0] * width, width)
    own = hidden_ref[:, pl.ds(start, width)].astype(jnp.float32)
    total = jnp.zeros((rows, 1), jnp.float32)
    squares = jnp.zeros((rows, 1), jnp.float32)
    for q in range(pieces):
        piece = alpha_res * own[:, q * narrow : (q + 1) * narrow]
        for k in range(top):
            at = (k * pieces + q) * rows
            piece = piece + weight_ref[:, k : k + 1] * chosen[at : at + rows, :]
        blend_ref[:, q * narrow : (q + 1) * narrow] = piece
        total = total + jnp.sum(piece, axis=1, keepdims=True)
        squares = squares + jnp.sum(piece * piece, axis=1, keepdims=True)
    lane = lax.broadcasted_iota(jnp.int32, stat_ref.shape, 1)
    stat_ref[...] = jnp.where(lane == 0, total, jnp.where(lane == 1, squares, 0.0))


def close_kernel(model_width, pair_ref, blend_ref, own_ref, other_ref, gain_ref, bias_ref, out_ref):
    width = blend_ref.shape[1]
    stats = (own_ref[...] + other_ref[...]) / model_width
    mean = stats[:, 0:1]
    spread = stats[:, 1:2] - mean * mean
    start = pl.multiple_of(pair_ref[0] * width, width)
    gain = gain_ref[1:2, pl.ds(start, width)]
    bias = bias_ref[1:2, pl.ds(start, width)]
    out_ref[...] = ((blend_ref[...] - mean) * lax.rsqrt(spread + eps_norm) * gain + bias).astype(jnp.bfloat16)


def small_call(kernel, shapes, specs, limit, flops):
    return pl.pallas_call(
        kernel,
        out_shape=shapes,
        in_specs=specs,
        out_specs=[in_vmem] * len(shapes),
        compiler_params=pltpu.CompilerParams(vmem_limit_bytes=limit * mib),
        cost_estimate=pl.CostEstimate(flops=flops, bytes_accessed=mib, transcendentals=0),
    )


def on_device(
    tokens,
    recurrent_state,
    query_weight,
    key_weight,
    decay_weight,
    value_weight,
    gate_weight,
    head_gain,
    output_weight,
    norm_gain,
    norm_bias,
    group_router,
    router_weight,
    routes,
    expert_gate,
    expert_up,
    expert_down,
):
    row_count, model_width = tokens.shape
    heads_here = recurrent_state.shape[1]
    key_dim = recurrent_state.shape[2]
    value_dim = recurrent_state.shape[3]

    tp_count = lax.axis_size("tp")
    ep_count = lax.axis_size("ep")
    pair_index = lax.axis_index("tp")
    pair = pair_index.reshape(1).astype(jnp.int32)
    own_part, key_rows, decay_rate, value_rows = mix(
        tokens, recurrent_state, query_weight, key_weight, decay_weight, value_weight, gate_weight,
        head_gain, output_weight,
    )
    capacity = 2 * max(1, row_count // router_weight.shape[1])
    pieces = cells // capacity
    lanes = jnp.tile(routes.T, (1, pieces))
    other_part = swapped(own_part)
    hidden, outgoing = small_call(
        functools.partial(send_kernel, tp_count, pieces),
        (
            jax.ShapeDtypeStruct((row_count, model_width), jnp.bfloat16),
            jax.ShapeDtypeStruct((ep_count * cells, model_width // pieces), jnp.bfloat16),
        ),
        [in_smem] + [in_vmem] * 7,
        8,
        20_000_000,
    )(pair, own_part, other_part, tokens, norm_gain, norm_bias, routes, lanes)
    group_count = group_router.shape[1]
    expert_count = router_weight.shape[1]
    per_group = expert_count // group_count
    top_count = routes.shape[1]
    group_logit = jnp.dot(hidden, group_router, preferred_element_type=jnp.float32)
    expert_logit = jnp.dot(hidden, router_weight, preferred_element_type=jnp.float32)
    chosen_group = routes[:, 0] // per_group
    group_hit = chosen_group[:, None] == jnp.arange(group_count, dtype=jnp.int32)[None, :]
    own_logit = jnp.sum(jnp.where(group_hit, group_logit, 0.0), axis=1, keepdims=True)
    group_share = 1.0 / jnp.sum(jnp.exp(group_logit - own_logit), axis=1)
    expert_hit = routes[:, :, None] == jnp.arange(expert_count, dtype=jnp.int32)[None, None, :]
    picked = jnp.sum(jnp.where(expert_hit, expert_logit[:, None, :], 0.0), axis=2)
    route_weight = group_share[:, None] * jax.nn.sigmoid(picked - picked[:, ::-1])
    late_decay, late_keys, late_values, outgoing = lax.optimization_barrier(
        (decay_rate, key_rows, value_rows, outgoing)
    )
    new_state = (
        late_decay.reshape(row_count, heads_here, key_dim, 1) * recurrent_state
        + late_keys.reshape(row_count, heads_here, key_dim, 1)
        * late_values.reshape(row_count, heads_here, 1, value_dim)
    )
    arrived = lax.all_to_all(
        outgoing.reshape(ep_count, cells, model_width // pieces), "ep", split_axis=0, concat_axis=0, tiled=True
    )
    arrived, new_state = lax.optimization_barrier((arrived, new_state))
    col_width = model_width // tp_count
    narrow = col_width // pieces
    device_count = ep_count * tp_count
    (results,) = small_call(
        functools.partial(expert_kernel, tp_count, pieces),
        (jax.ShapeDtypeStruct((device_count * cells, narrow), jnp.bfloat16),),
        [in_vmem] * 4,
        16,
        100_000_000,
    )(arrived.reshape(ep_count * cells, model_width // pieces), expert_gate, expert_up, expert_down)
    returned = lax.all_to_all(
        results.reshape(device_count, cells, narrow), ("ep", "tp"), split_axis=0, concat_axis=0, tiled=True
    )
    blended, own_stats = small_call(
        functools.partial(blend_kernel, pieces),
        (
            jax.ShapeDtypeStruct((row_count, col_width), jnp.float32),
            jax.ShapeDtypeStruct((row_count, 128), jnp.float32),
        ),
        [in_smem] + [in_vmem] * 5,
        8,
        20_000_000,
    )(pair, returned.reshape(device_count * cells, narrow), routes, lanes, route_weight, hidden)
    other_stats = swapped(own_stats)
    (new_tokens,) = small_call(
        functools.partial(close_kernel, model_width),
        (jax.ShapeDtypeStruct((row_count, col_width), jnp.bfloat16),),
        [in_smem] + [in_vmem] * 5,
        8,
        1_000_000,
    )(pair, blended, own_stats, other_stats, norm_gain, norm_bias)
    return (new_tokens, new_state)


def solution(mesh):
    in_specs = (
        P("ep", None),
        P("ep", "tp", None, None),
        P(None, "tp"),
        P(None, "tp"),
        P(None, "tp"),
        P(None, "tp"),
        P(None, "tp"),
        P(),
        P("tp", None),
        P(),
        P(),
        P(),
        P(),
        P("ep", None),
        P(("ep", "tp"), None, None),
        P(("ep", "tp"), None, None),
        P(("ep", "tp"), None, None),
    )
    out_specs = (P("ep", "tp"), P("ep", "tp", None, None))
    return jax.shard_map(
        on_device, mesh=mesh, in_specs=in_specs, out_specs=out_specs, check_vma=False
    )
```

time: 49.9 us -> 52.6 us (1.054)
  matrix products: 12.6 us -> 0.29 us
  local copies, waits for them, and re-layouts: 2.54 us -> 13.8 us
  Pallas kernels: 0 us -> 8.1 us
  other arithmetic: 9.76 us -> 4.65 us
  starting transfers between devices: 11.2 us -> 11.9 us
    dot_general x9 -> x0, matrix products: 12.3 us -> none  [the longest x4 5.4 us: project(): return jnp.dot(tokens, weight, preferred_element_type=jnp.float32)]
    unnamed x28 -> x37, local copies, waits for them, and re-layouts: 0.17 us -> 12.3 us
    pallas_call x0 -> x5, Pallas kernels: none -> 8.1 us  [the longest x1 4.21 us: mix(): pl.pallas_call(functools.partial(mix_kernel, key_dim, value_dim), out_sha...]
    reduce_sum x8 -> x0, other arithmetic: 3.58 us -> none  [the longest x1 2.62 us: on_device(): jnp.sum((queries * decay_rate)[..., None] * recurrent_state, axis=2)]
    reshape x7 -> x0, local copies, waits for them, and re-layouts: 1.73 us -> none  [the longest x1 0.77 us: on_device(): halves = jnp.transpose(results.reshape(ep_count, local_experts * capacity...]
    mul x3, local copies, waits for them, and re-layouts: 0.17 us -> 1.25 us  [the longest x2 0.64 us: on_device(): late_keys.reshape(row_count, heads_here, key_dim, 1)]
    convert_element_type x4 -> x0, other arithmetic: 0.97 us -> none  [the longest x1 0.7 us: on_device(): new_tokens = ((blended - row_mean[:, None]) * lax.rsqrt(spread[:, None] +...]
    ppermute x2, waiting for transfers between devices: 0.95 us -> 1.67 us  [swapped(): lax.ppermute(values, 'tp', [(i, (i + 1) % count) for i in range(count)])]
  transfers between devices with their start and end apart: 4 -> 4, of which waited for: 3 -> 4; matrix products, arithmetic and copies ran while one was open for 13% -> 10% of each run, Pallas kernels for 0% -> 0%
where the time goes in v2:
time: 52.6 us; the launch traced here: 52.1 us
  local copies, waits for them, and re-layouts  13.8 us (26%)
  waiting for transfers between devices  12.5 us (24%)
  starting transfers between devices  11.9 us (23%)
  Pallas kernels  8.1 us (15%)
  other arithmetic  4.65 us (9%)
  between operations  0.77 us (1%)
    unnamed x37, local copies, waits for them, and re-layouts  12.3 us
    all_to_all x1, starting transfers between devices, on_device(): lax.all_to_all(outgoing.reshape(ep_count, cells, model_width // pieces),...  8.2 us
    all_to_all x1, waiting for transfers between devices, on_device(): lax.all_to_all(results.reshape(device_count, cells, narrow), ('ep', 'tp')...  7.82 us
    add x1, other arithmetic, on_device(): late_decay.reshape(row_count, heads_here, key_dim, 1) * recurrent_state  4.39 us
    pallas_call x1, Pallas kernels, mix(): pl.pallas_call(functools.partial(mix_kernel, key_dim, value_dim), out_sha...  4.21 us
    all_to_all x1, waiting for transfers between devices, on_device(): lax.all_to_all(outgoing.reshape(ep_count, cells, model_width // pieces),...  3.03 us
    all_to_all x1, starting transfers between devices, on_device(): lax.all_to_all(results.reshape(device_count, cells, narrow), ('ep', 'tp')...  2.89 us
    ppermute x2, waiting for transfers between devices, swapped(): lax.ppermute(values, 'tp', [(i, (i + 1) % count) for i in range(count)])  1.67 us
  transfers between devices with their start and end apart: 4, of which 4 were waited for; matrix products, arithmetic and copies ran while one was open for 10% of the time, Pallas kernels for 0%

profile of v2, /device:TPU:0, one launch (start us, length us, event | category | flops | bytes accessed | tf_op | source)
XLA Modules:
  0.0 52.1 jit_solution(15010809840098775908)
XLA Ops:
  0.6 0.0 copy-start
  0.7 0.0 copy-start.1
  0.7 2.2 %copy-done.1 = f32[16,2,128,256]{3,2,1,0:T(8,128)S(1)} copy-done((f32[16,2,128,256]{3,2,1,0:T(8,128)S(1)}, f32[16,2,128,256]{3,2,1,0:T(8,128)}, u32[]{:S(2)}) %copy-start.1) | copy-done | bytes 4194328
  2.9 1.6 %copy-done.2 = bf16[2048,512]{1,0:T(8,128)(2,1)S(1)} copy-done((bf16[2048,512]{1,0:T(8,128)(2,1)S(1)}, bf16[2048,512]{1,0:T(8,128)(2,1)}, u32[]{:S(2)}) %copy-start.2) | copy-done | bytes 2097176
  4.5 1.6 %copy-done.3 = bf16[2048,512]{1,0:T(8,128)(2,1)S(1)} copy-done((bf16[2048,512]{1,0:T(8,128)(2,1)S(1)}, bf16[2048,512]{1,0:T(8,128)(2,1)}, u32[]{:S(2)}) %copy-start.3) | copy-done | bytes 2097176
  6.1 1.6 %copy-done.4 = bf16[512,2048]{1,0:T(8,128)(2,1)S(1)} copy-done((bf16[512,2048]{1,0:T(8,128)(2,1)S(1)}, bf16[512,2048]{1,0:T(8,128)(2,1)}, u32[]{:S(2)}) %copy-start.4) | copy-done | bytes 2097176
  7.7 1.2 %copy-done.8 = bf16[2048,256]{1,0:T(8,128)(2,1)S(1)} copy-done((bf16[2048,256]{1,0:T(8,128)(2,1)S(1)}, bf16[2048,256]{1,0:T(8,128)(2,1)}, u32[]{:S(2)}) %copy-start.8) | copy-done | bytes 1048600
  8.9 1.2 %copy-done.9 = bf16[2048,256]{1,0:T(8,128)(2,1)S(1)} copy-done((bf16[2048,256]{1,0:T(8,128)(2,1)S(1)}, bf16[2048,256]{1,0:T(8,128)(2,1)}, u32[]{:S(2)}) %copy-start.9) | copy-done | bytes 1048600
  10.1 1.2 %copy-done.10 = bf16[2048,256]{1,0:T(8,128)(2,1)S(1)} copy-done((bf16[2048,256]{1,0:T(8,128)(2,1)S(1)}, bf16[2048,256]{1,0:T(8,128)(2,1)}, u32[]{:S(2)}) %copy-start.10) | copy-done | bytes 1048600
  11.3 0.8 %copy-done.11 = bf16[16,2048]{1,0:T(8,128)(2,1)S(1)} copy-done((bf16[16,2048]{1,0:T(8,128)(2,1)S(1)}, bf16[16,2048]{1,0:T(8,128)(2,1)}, u32[]{:S(2)}) %copy-start.11) | copy-done | bytes 65560
  12.2 0.7 %copy-done.15 = f32[256]{0:T(256)S(1)} copy-done((f32[256]{0:T(256)S(1)}, f32[256]{0:T(256)}, u32[]{:S(2)}) %copy-start.15) | copy-done | bytes 1048
  12.9 0.0 copy-start.17
  12.9 4.2 %shard_map.176 = (bf16[16,2048]{1,0:T(8,128)(2,1)S(1)}, f32[16,256]{1,0:T(8,128)S(1)}, f32[16,256]{1,0:T(8,128)S(1)}, f32[16,512]{1,0:T(8,128)S(1)}) custom-call(bf16[16,2048]{1,0:T(8,128)(2,1)S(1)} %copy-done.11, f32[1,256]{1,0:T(1,128)S(1)} %bitcast.15, bf16[2048,256]{1,0:T(8,128)(2,1)S(1)} %copy-done.8, bf16[2048,256]{1,0:T(8,128)(2,1)S(1)} %copy-done.9, ...), custom_call_target="tpu_custom_call" | custom-call | flops 200000000 | bytes 14680064 | tf_op jit(solution)/shard_map/pallas_call | solution.py:79
  17.1 0.6 %collective-permute-start = (bf16[16,2048]{1,0:T(8,128)(2,1)S(1)}, bf16[16,2048]{1,0:T(8,128)(2,1)S(1)}, u32[]{:S(2)}, u32[]{:S(2)}) collective-permute-start(bf16[16,2048]{1,0:T(8,128)(2,1)S(1)} %get-tuple-element.19.own_ref), channel_id=1, source_target_pairs={{0,1},{1,0},{2,3},{3,2},{4,5},{5,4},{6,7},{7,6},{8,9},{9,8},{10,11... | collective-permute-start | bytes 196616 | tf_op jit(solution)/shard_map/ppermute | solution.py:21
  17.6 0.0 copy-done.16
  17.7 0.1 copy.26.routes_ref
  17.7 0.1 tile.10.lanes_ref
  17.8 0.7 %collective-permute-done.other_ref = bf16[16,2048]{1,0:T(8,128)(2,1)S(1)} collective-permute-done((bf16[16,2048]{1,0:T(8,128)(2,1)S(1)}, bf16[16,2048]{1,0:T(8,128)(2,1)S(1)}, u32[]{:S(2)}, u32[]{:S(2)}) %collective-permute-start) | collective-permute-done | bytes 65568 | tf_op jit(solution)/shard_map/ppermute | solution.py:21
  18.5 0.0 copy-done.12
  18.5 0.0 copy-done.13
  18.5 0.0 copy-done.14
  18.6 1.0 %shard_map.177 = (bf16[16,2048]{1,0:T(8,128)(2,1)S(1)}, bf16[128,512]{1,0:T(8,128)(2,1)}) custom-call(s32[1]{0:T(128)} %bitcast.pair_ref, bf16[16,2048]{1,0:T(8,128)(2,1)S(1)} %get-tuple-element.19.own_ref, bf16[16,2048]{1,0:T(8,128)(2,1)S(1)} %collective-permute-done.other_ref, bf16[16,2048]{1,0:T(8,128)(2,1)S(1)} %copy-done.12, f32[2,2048]{1,0:T(2,128)S(1)} %copy-done.13, ...), custom_call_target="tpu_custom_call" | custom-call | flops 20000000 | bytes 1048576 | tf_op jit(solution)/shard_map/pallas_call | solution.py:262
  19.6 0.6 %mul.35 = f32[16,2,128]{2,1,0:T(2,128)} reshape(f32[16,256]{1,0:T(8,128)S(1)} %get-tuple-element.22) | data formatting | bytes 32768 | tf_op jit(solution)/shard_map/mul | solution.py:289
  20.2 0.6 %mul.38 = f32[16,2,128]{2,1,0:T(2,128)} reshape(f32[16,256]{1,0:T(8,128)S(1)} %get-tuple-element.23) | data formatting | bytes 32768 | tf_op jit(solution)/shard_map/mul | solution.py:290
  20.8 8.2 %all-to-all-start = ((bf16[16,8,512]{2,1,0:T(8,128)(2,1)}), bf16[16,8,512]{2,1,0:T(8,128)(2,1)S(1)}, u32[]{:S(2)}, u32[]{:S(2)}) async-start(bf16[16,8,512]{2,1,0:T(8,128)(2,1)} %bitcast.3), calls=%async_computation | async-start | bytes 262144 | tf_op jit(solution)/shard_map/all_to_all | solution.py:293
  29.1 0.0 copy-done.17
  29.1 0.1 select_reduce_fusion.1
  29.2 0.0 copy-start.5
  29.3 0.0 copy-start.6
  29.3 0.0 copy-start.7
  29.3 4.4 %multiply_add_fusion = f32[16,2,128,256]{3,2,1,0:T(8,128)} fusion(f32[16,2,128,256]{3,2,1,0:T(8,128)} %state.1, f32[16,2,256]{2,1,0:T(2,128)S(1)} %mul.40, f32[16,2,128]{2,1,0:T(2,128)} %mul.38, f32[16,2,128]{2,1,0:T(2,128)} %mul.35), kind=kLoop, calls=%fused_computation | loop fusion | flops 3145728 | bytes 8454144 | tf_op jit(solution)/shard_map/add | solution.py:289
  33.7 0.0 copy-done
  33.7 0.1 fusion.1
  33.8 3.0 %all-to-all-done = bf16[16,8,512]{2,1,0:T(8,128)(2,1)S(1)} async-done(((bf16[16,8,512]{2,1,0:T(8,128)(2,1)}), bf16[16,8,512]{2,1,0:T(8,128)(2,1)S(1)}, u32[]{:S(2)}, u32[]{:S(2)}) %all-to-all-start) | async-done | bytes 131104 | tf_op jit(solution)/shard_map/all_to_all | solution.py:293
  36.9 0.0 copy-done.5
  36.9 0.0 copy-done.6
  36.9 0.0 copy-done.7
  36.9 1.6 %shard_map.178 = bf16[256,256]{1,0:T(8,128)(2,1)} custom-call(bf16[128,512]{1,0:T(8,128)(2,1)S(1)} %bitcast.14, bf16[1,2048,256]{2,1,0:T(8,128)(2,1)S(1)} %copy-done.5, bf16[1,2048,256]{2,1,0:T(8,128)(2,1)S(1)} %copy-done.6, bf16[1,256,2048]{2,1,0:T(8,128)(2,1)S(1)} %copy-done.7), custom_call_target="tpu_custom_call" | custom-call | flops 100000000 | bytes 1048576 | tf_op jit(solution)/shard_map/pallas_call | solution.py:300
  38.5 2.9 %all-to-all-start.1 = ((bf16[32,8,256]{2,1,0:T(8,128)(2,1)}), bf16[32,8,256]{2,1,0:T(8,128)(2,1)S(1)}, u32[]{:S(2)}, u32[]{:S(2)}) async-start(bf16[32,8,256]{2,1,0:T(8,128)(2,1)} %bitcast.5), calls=%async_computation.1 | async-start | bytes 262144 | tf_op jit(solution)/shard_map/all_to_all | solution.py:307
  41.4 0.2 select_reduce_fusion
  41.6 0.1 copy.28
  41.6 0.1 rev.3
  41.7 0.1 divide_multiply_fusion.weight_ref
  41.8 7.8 %all-to-all-done.1 = bf16[32,8,256]{2,1,0:T(8,128)(2,1)S(1)} async-done(((bf16[32,8,256]{2,1,0:T(8,128)(2,1)}), bf16[32,8,256]{2,1,0:T(8,128)(2,1)S(1)}, u32[]{:S(2)}, u32[]{:S(2)}) %all-to-all-start.1) | async-done | bytes 131104 | tf_op jit(solution)/shard_map/all_to_all | solution.py:307
  49.6 0.5 shard_map.179
  50.1 0.3 collective-permute-start.1
  50.3 1.0 %collective-permute-done.1.other_ref = f32[16,128]{1,0:T(8,128)S(1)} collective-permute-done((f32[16,128]{1,0:T(8,128)S(1)}, f32[16,128]{1,0:T(8,128)S(1)}, u32[]{:S(2)}, u32[]{:S(2)}) %collective-permute-start.1) | collective-permute-done | bytes 8224 | tf_op jit(solution)/shard_map/ppermute | solution.py:21
  51.3 0.8 %shard_map.180 = bf16[16,1024]{1,0:T(8,128)(2,1)} custom-call(s32[1]{0:T(128)} %bitcast.pair_ref, f32[16,1024]{1,0:T(8,128)S(1)} %get-tuple-element.27.blend_ref, f32[16,128]{1,0:T(8,128)S(1)} %get-tuple-element.28.own_ref, f32[16,128]{1,0:T(8,128)S(1)} %collective-permute-done.1.other_ref, f32[2,2048]{1,0:T(2,128)S(1)} %copy-done.13, f32[2,2048]{1,0:T(2,128)S(1)} %copy-done.14), custom_call_target="tpu_custom_call" | custom-call | flops 1000000 | bytes 1048576 | tf_op jit(solution)/shard_map/pallas_call | solution.py:321
  (17 shorter events, 0.1 us)
Async XLA Ops:
  0.6 33.0 %copy-start = (bf16[2048,32]{0,1:T(8,128)(2,1)S(1)}, bf16[2048,32]{0,1:T(8,128)(2,1)}, u32[]{:S(2)}) copy-start(bf16[2048,32]{0,1:T(8,128)(2,1)} %param.29) | copy-start | bytes 393220
  0.7 2.2 %copy-start.1 = (f32[16,2,128,256]{3,2,1,0:T(8,128)S(1)}, f32[16,2,128,256]{3,2,1,0:T(8,128)}, u32[]{:S(2)}) copy-start(f32[16,2,128,256]{3,2,1,0:T(8,128)} %state.1) | copy-start | bytes 12582916
  2.9 1.6 %copy-start.2 = (bf16[2048,512]{1,0:T(8,128)(2,1)S(1)}, bf16[2048,512]{1,0:T(8,128)(2,1)}, u32[]{:S(2)}) copy-start(bf16[2048,512]{1,0:T(8,128)(2,1)} %wv.1) | copy-start | bytes 6291460
  4.5 1.6 %copy-start.3 = (bf16[2048,512]{1,0:T(8,128)(2,1)S(1)}, bf16[2048,512]{1,0:T(8,128)(2,1)}, u32[]{:S(2)}) copy-start(bf16[2048,512]{1,0:T(8,128)(2,1)} %wg.1) | copy-start | bytes 6291460
  6.1 1.6 %copy-start.4 = (bf16[512,2048]{1,0:T(8,128)(2,1)S(1)}, bf16[512,2048]{1,0:T(8,128)(2,1)}, u32[]{:S(2)}) copy-start(bf16[512,2048]{1,0:T(8,128)(2,1)} %wo.1) | copy-start | bytes 6291460
  7.7 1.2 %copy-start.8 = (bf16[2048,256]{1,0:T(8,128)(2,1)S(1)}, bf16[2048,256]{1,0:T(8,128)(2,1)}, u32[]{:S(2)}) copy-start(bf16[2048,256]{1,0:T(8,128)(2,1)} %wq.1) | copy-start | bytes 3145732
  8.9 1.2 %copy-start.9 = (bf16[2048,256]{1,0:T(8,128)(2,1)S(1)}, bf16[2048,256]{1,0:T(8,128)(2,1)}, u32[]{:S(2)}) copy-start(bf16[2048,256]{1,0:T(8,128)(2,1)} %wd.1) | copy-start | bytes 3145732
  10.1 1.2 %copy-start.10 = (bf16[2048,256]{1,0:T(8,128)(2,1)S(1)}, bf16[2048,256]{1,0:T(8,128)(2,1)}, u32[]{:S(2)}) copy-start(bf16[2048,256]{1,0:T(8,128)(2,1)} %wk.1) | copy-start | bytes 3145732
  11.3 0.8 %copy-start.11 = (bf16[16,2048]{1,0:T(8,128)(2,1)S(1)}, bf16[16,2048]{1,0:T(8,128)(2,1)}, u32[]{:S(2)}) copy-start(bf16[16,2048]{1,0:T(8,128)(2,1)} %tokens_ref.3) | copy-start | bytes 196612
  12.2 0.7 %copy-start.15 = (f32[256]{0:T(256)S(1)}, f32[256]{0:T(256)}, u32[]{:S(2)}) copy-start(f32[256]{0:T(256)} %param.24) | copy-start | bytes 3076
  12.8 4.8 %copy-start.16 = (s32[16,2]{0,1:T(2,128)S(1)}, s32[16,2]{0,1:T(2,128)}, u32[]{:S(2)}) copy-start(s32[16,2]{0,1:T(2,128)} %param.30) | copy-start | bytes 388
  12.8 5.7 %copy-start.12 = (bf16[16,2048]{1,0:T(8,128)(2,1)S(1)}, bf16[16,2048]{1,0:T(8,128)(2,1)}, u32[]{:S(2)}) copy-start(bf16[16,2048]{1,0:T(8,128)(2,1)} %tokens_ref.3) | copy-start | bytes 196612
  12.9 5.7 %copy-start.13 = (f32[2,2048]{1,0:T(2,128)S(1)}, f32[2,2048]{1,0:T(2,128)}, u32[]{:S(2)}) copy-start(f32[2,2048]{1,0:T(2,128)} %gain_ref.3) | copy-start | bytes 49156
  12.9 5.7 %copy-start.14 = (f32[2,2048]{1,0:T(2,128)S(1)}, f32[2,2048]{1,0:T(2,128)}, u32[]{:S(2)}) copy-start(f32[2,2048]{1,0:T(2,128)} %bias_ref.3) | copy-start | bytes 49156
  12.9 16.2 %copy-start.17 = (bf16[2048,4]{0,1:T(4,128)(2,1)S(1)}, bf16[2048,4]{0,1:T(4,128)(2,1)}, u32[]{:S(2)}) copy-start(bf16[2048,4]{0,1:T(4,128)(2,1)} %param.28) | copy-start | bytes 49156
  17.1 1.5 %collective-permute-start = (bf16[16,2048]{1,0:T(8,128)(2,1)S(1)}, bf16[16,2048]{1,0:T(8,128)(2,1)S(1)}, u32[]{:S(2)}, u32[]{:S(2)}) collective-permute-start(bf16[16,2048]{1,0:T(8,128)(2,1)S(1)} %get-tuple-element.19.own_ref), channel_id=1, source_target_pairs={{0,1},{1,0},{2,3},{3,2},{4,5},{5,4},{6,7},{7,6},{8,9},{9,8},{10,11... | collective-permute-start | bytes 196616 | tf_op jit(solution)/shard_map/ppermute | solution.py:21
  20.8 16.0 %all-to-all-start = ((bf16[16,8,512]{2,1,0:T(8,128)(2,1)}), bf16[16,8,512]{2,1,0:T(8,128)(2,1)S(1)}, u32[]{:S(2)}, u32[]{:S(2)}) async-start(bf16[16,8,512]{2,1,0:T(8,128)(2,1)} %bitcast.3), calls=%async_computation | async-start | bytes 262144 | tf_op jit(solution)/shard_map/all_to_all | solution.py:293
  29.2 7.6 %copy-start.5 = (bf16[1,2048,256]{2,1,0:T(8,128)(2,1)S(1)}, bf16[1,2048,256]{2,1,0:T(8,128)(2,1)}, u32[]{:S(2)}) copy-start(bf16[1,2048,256]{2,1,0:T(8,128)(2,1)} %gate_ref.1) | copy-start | bytes 3145732
  29.3 7.6 %copy-start.6 = (bf16[1,2048,256]{2,1,0:T(8,128)(2,1)S(1)}, bf16[1,2048,256]{2,1,0:T(8,128)(2,1)}, u32[]{:S(2)}) copy-start(bf16[1,2048,256]{2,1,0:T(8,128)(2,1)} %up_ref.1) | copy-start | bytes 3145732
  29.3 7.6 %copy-start.7 = (bf16[1,256,2048]{2,1,0:T(8,128)(2,1)S(1)}, bf16[1,256,2048]{2,1,0:T(8,128)(2,1)}, u32[]{:S(2)}) copy-start(bf16[1,256,2048]{2,1,0:T(8,128)(2,1)} %down_ref.1) | copy-start | bytes 3145732
  38.5 11.1 %all-to-all-start.1 = ((bf16[32,8,256]{2,1,0:T(8,128)(2,1)}), bf16[32,8,256]{2,1,0:T(8,128)(2,1)S(1)}, u32[]{:S(2)}, u32[]{:S(2)}) async-start(bf16[32,8,256]{2,1,0:T(8,128)(2,1)} %bitcast.5), calls=%async_computation.1 | async-start | bytes 262144 | tf_op jit(solution)/shard_map/all_to_all | solution.py:307
  50.1 1.2 %collective-permute-start.1 = (f32[16,128]{1,0:T(8,128)S(1)}, f32[16,128]{1,0:T(8,128)S(1)}, u32[]{:S(2)}, u32[]{:S(2)}) collective-permute-start(f32[16,128]{1,0:T(8,128)S(1)} %get-tuple-element.28.own_ref), channel_id=1, source_target_pairs={{0,1},{1,0},{2,3},{3,2},{4,5},{5,4},{6,7},{7,6},{8,9},{9,8},{10,11... | collective-permute-start | bytes 24584 | tf_op jit(solution)/shard_map/ppermute | solution.py:21

commit v3 on v2

--- a/solution.py
+++ b/solution.py
@@ -93,7 +93,7 @@
             pltpu.VMEM((heads, rows, value_dim), f32),
             pltpu.SemaphoreType.DMA((7,)),
         ],
-        compiler_params=pltpu.CompilerParams(vmem_limit_bytes=28 * mib),
+        compiler_params=pltpu.CompilerParams(vmem_limit_bytes=60 * mib),
         cost_estimate=pl.CostEstimate(flops=200_000_000, bytes_accessed=14 * mib, transcendentals=0),
     )(tokens, gain.reshape(1, -1), wq, wd, wk, wv, wg, state, wo)
 

time: 52.6 us -> 47.7 us (0.907)
  local copies, waits for them, and re-layouts: 13.8 us -> 4.66 us
  Pallas kernels: 8.1 us -> 10.9 us
  waiting for transfers between devices: 12.5 us -> 10.1 us
  other arithmetic: 4.65 us -> 6.62 us
  starting transfers between devices: 11.9 us -> 13.1 us
  matrix products: 0.29 us -> 0.91 us
    unnamed x37 -> x21, local copies, waits for them, and re-layouts: 12.3 us -> 0.97 us
    pallas_call x1, Pallas kernels: 4.21 us -> 7.08 us  [mix(): pl.pallas_call(functools.partial(mix_kernel, key_dim, value_dim), out_sha...]
    mul x2, local copies, waits for them, and re-layouts: 0.64 us -> 2.11 us  [on_device(): late_keys.reshape(row_count, heads_here, key_dim, 1)]
    all_to_all x1, waiting for transfers between devices: 7.82 us -> 6.45 us  [on_device(): lax.all_to_all(results.reshape(device_count, cells, narrow), ('ep', 'tp')...]
    all_to_all x1, waiting for transfers between devices: 3.03 us -> 1.82 us  [on_device(): lax.all_to_all(outgoing.reshape(ep_count, cells, model_width // pieces),...]
    all_to_all x1, starting transfers between devices: 2.89 us -> 4.08 us  [on_device(): lax.all_to_all(results.reshape(device_count, cells, narrow), ('ep', 'tp')...]
    mul x1, local copies, waits for them, and re-layouts: 0.61 us -> 1.33 us  [on_device(): late_decay.reshape(row_count, heads_here, key_dim, 1) * recurrent_state]
    reduce_sum x1, other arithmetic: 0.16 us -> 0.85 us  [on_device(): jnp.sum(jnp.where(expert_hit, expert_logit[:, None, :], 0.0), axis=2)]
  transfers between devices with their start and end apart: 4 -> 4, of which waited for: 4 -> 4; matrix products, arithmetic and copies ran while one was open for 10% -> 17% of each run, Pallas kernels for 0% -> 0%
where the time goes in v3:
time: 47.7 us; the launch traced here: 47.2 us
  starting transfers between devices  13.1 us (27%)
  Pallas kernels  10.9 us (23%)
  waiting for transfers between devices  10.1 us (21%)
  other arithmetic  6.62 us (14%)
  local copies, waits for them, and re-layouts  4.66 us (10%)
  matrix products  0.91 us (2%)
  between operations  0.78 us (2%)
    all_to_all x1, starting transfers between devices, on_device(): lax.all_to_all(outgoing.reshape(ep_count, cells, model_width // pieces),...  8.2 us
    pallas_call x1, Pallas kernels, mix(): pl.pallas_call(functools.partial(mix_kernel, key_dim, value_dim), out_sha...  7.08 us
    all_to_all x1, waiting for transfers between devices, on_device(): lax.all_to_all(results.reshape(device_count, cells, narrow), ('ep', 'tp')...  6.45 us
    add x1, other arithmetic, on_device(): late_decay.reshape(row_count, heads_here, key_dim, 1) * recurrent_state  4.4 us
    all_to_all x1, starting transfers between devices, on_device(): lax.all_to_all(results.reshape(device_count, cells, narrow), ('ep', 'tp')...  4.08 us
    mul x2, local copies, waits for them, and re-layouts, on_device(): late_keys.reshape(row_count, heads_here, key_dim, 1)  2.11 us
    ppermute x2, waiting for transfers between devices, swapped(): lax.ppermute(values, 'tp', [(i, (i + 1) % count) for i in range(count)])  1.88 us
    all_to_all x1, waiting for transfers between devices, on_device(): lax.all_to_all(outgoing.reshape(ep_count, cells, model_width // pieces),...  1.82 us
  transfers between devices with their start and end apart: 4, of which 4 were waited for; matrix products, arithmetic and copies ran while one was open for 17% of the time, Pallas kernels for 0%

profile of v3, /device:TPU:0, one launch (start us, length us, event | category | flops | bytes accessed | tf_op | source)
XLA Modules:
  0.0 47.2 jit_solution(2939387222682522861)
XLA Ops:
  0.6 0.0 copy-start
  0.7 0.0 copy-start.8
  0.7 0.0 copy-start.4
  0.7 0.0 copy-start.6
  0.7 0.0 copy-start.7
  0.7 0.0 copy-start.9
  0.7 7.1 %shard_map.176 = (bf16[16,2048]{1,0:T(8,128)(2,1)}, f32[16,256]{1,0:T(8,128)}, f32[16,256]{1,0:T(8,128)}, f32[16,512]{1,0:T(8,128)}) custom-call(bf16[16,2048]{1,0:T(8,128)(2,1)} %tokens_ref.3, f32[1,256]{1,0:T(1,128)} %bitcast.16, bf16[2048,256]{1,0:T(8,128)(2,1)} %wq.1, bf16[2048,256]{1,0:T(8,128)(2,1)} %wd.1, bf16[2048,256]{1,0:T(8,128)(2,1)} %wk.1, ...), custom_call_target="tpu_custom_call" | custom-call | flops 200000000 | bytes 14680064 | tf_op jit(solution)/shard_map/pallas_call | solution.py:79
  7.8 0.6 %collective-permute-start = (bf16[16,2048]{1,0:T(8,128)(2,1)}, bf16[16,2048]{1,0:T(8,128)(2,1)S(1)}, u32[]{:S(2)}, u32[]{:S(2)}) collective-permute-start(bf16[16,2048]{1,0:T(8,128)(2,1)} %get-tuple-element.19.own_ref), channel_id=1, source_target_pairs={{0,1},{1,0},{2,3},{3,2},{4,5},{5,4},{6,7},{7,6},{8,9},{9,8},{10,11... | collective-permute-start | bytes 196616 | tf_op jit(solution)/shard_map/ppermute | solution.py:21
  8.4 0.0 copy-done.8
  8.4 0.1 copy.26.routes_ref
  8.5 0.1 tile.10.lanes_ref
  8.5 0.9 %collective-permute-done.other_ref = bf16[16,2048]{1,0:T(8,128)(2,1)S(1)} collective-permute-done((bf16[16,2048]{1,0:T(8,128)(2,1)}, bf16[16,2048]{1,0:T(8,128)(2,1)S(1)}, u32[]{:S(2)}, u32[]{:S(2)}) %collective-permute-start) | collective-permute-done | bytes 65568 | tf_op jit(solution)/shard_map/ppermute | solution.py:21
  9.5 0.0 copy-done.4
  9.5 0.0 copy-done.6
  9.5 0.0 copy-done.7
  9.5 0.0 copy-start.5
  9.5 0.8 %copy-done.5 = bf16[16,2048]{1,0:T(8,128)(2,1)S(1)} copy-done((bf16[16,2048]{1,0:T(8,128)(2,1)S(1)}, bf16[16,2048]{1,0:T(8,128)(2,1)}, u32[]{:S(2)}) %copy-start.5) | copy-done | bytes 65560
  10.3 1.0 %shard_map.177 = (bf16[16,2048]{1,0:T(8,128)(2,1)S(1)}, bf16[128,512]{1,0:T(8,128)(2,1)}) custom-call(s32[1]{0:T(128)} %bitcast.pair_ref, bf16[16,2048]{1,0:T(8,128)(2,1)S(1)} %copy-done.5, bf16[16,2048]{1,0:T(8,128)(2,1)S(1)} %collective-permute-done.other_ref, bf16[16,2048]{1,0:T(8,128)(2,1)S(1)} %copy-done.4, f32[2,2048]{1,0:T(2,128)S(1)} %copy-done.6, ...), custom_call_target="tpu_custom_call" | custom-call | flops 20000000 | bytes 1048576 | tf_op jit(solution)/shard_map/pallas_call | solution.py:262
  11.3 0.8 %mul.40 = f32[16,2,256]{2,1,0:T(2,128)S(1)} reshape(f32[16,512]{1,0:T(8,128)} %get-tuple-element.24) | data formatting | bytes 65536 | tf_op jit(solution)/shard_map/mul | solution.py:290
  12.1 1.3 %mul.35 = f32[16,2,128]{2,1,0:T(2,128)} reshape(f32[16,256]{1,0:T(8,128)} %get-tuple-element.22) | data formatting | bytes 32768 | tf_op jit(solution)/shard_map/mul | solution.py:289
  13.5 1.3 %mul.38 = f32[16,2,128]{2,1,0:T(2,128)} reshape(f32[16,256]{1,0:T(8,128)} %get-tuple-element.23) | data formatting | bytes 32768 | tf_op jit(solution)/shard_map/mul | solution.py:290
  14.8 8.2 %all-to-all-start = ((bf16[16,8,512]{2,1,0:T(8,128)(2,1)}), bf16[16,8,512]{2,1,0:T(8,128)(2,1)S(1)}, u32[]{:S(2)}, u32[]{:S(2)}) async-start(bf16[16,8,512]{2,1,0:T(8,128)(2,1)} %bitcast.3), calls=%async_computation | async-start | bytes 262144 | tf_op jit(solution)/shard_map/all_to_all | solution.py:293
  23.0 0.0 copy-done.9
  23.0 0.1 select_reduce_fusion.1
  23.2 0.0 copy-start.1
  23.2 0.0 copy-start.2
  23.2 0.0 copy-start.3
  23.2 4.4 %multiply_add_fusion = f32[16,2,128,256]{3,2,1,0:T(8,128)} fusion(f32[16,2,128,256]{3,2,1,0:T(8,128)} %state.1, f32[16,2,256]{2,1,0:T(2,128)S(1)} %mul.40, f32[16,2,128]{2,1,0:T(2,128)} %mul.38, f32[16,2,128]{2,1,0:T(2,128)} %mul.35), kind=kLoop, calls=%fused_computation | loop fusion | flops 3145728 | bytes 8454144 | tf_op jit(solution)/shard_map/add | solution.py:289
  27.6 0.6 %broadcast_divide_fusion = f32[16]{0:T(128)} fusion(f32[16]{0:T(128)S(1)} %exponential_reduce_fusion), kind=kLoop, calls=%fused_computation.12 | loop fusion | flops 16 | bytes 128 | tf_op jit(solution)/shard_map/div | solution.py:281
  28.2 0.0 copy-done
  28.2 0.8 %fusion.1 = f32[16,32]{1,0:T(8,128)} fusion(bf16[16,2048]{1,0:T(8,128)(2,1)S(1)} %get-tuple-element.26.hidden_ref, bf16[2048,32]{0,1:T(8,128)(2,1)S(1)} %copy-done), kind=kOutput, calls=%fused_computation.13 | convolution fusion | flops 2097152 | bytes 198656 | tf_op jit(solution)/shard_map/dot_general | solution.py:277
  29.0 1.8 %all-to-all-done = bf16[16,8,512]{2,1,0:T(8,128)(2,1)S(1)} async-done(((bf16[16,8,512]{2,1,0:T(8,128)(2,1)}), bf16[16,8,512]{2,1,0:T(8,128)(2,1)S(1)}, u32[]{:S(2)}, u32[]{:S(2)}) %all-to-all-start) | async-done | bytes 131104 | tf_op jit(solution)/shard_map/all_to_all | solution.py:293
  30.8 0.0 copy-done.1
  30.8 0.0 copy-done.2
  30.8 0.0 copy-done.3
  30.8 1.6 %shard_map.178 = bf16[256,256]{1,0:T(8,128)(2,1)} custom-call(bf16[128,512]{1,0:T(8,128)(2,1)S(1)} %bitcast.14, bf16[1,2048,256]{2,1,0:T(8,128)(2,1)S(1)} %copy-done.1, bf16[1,2048,256]{2,1,0:T(8,128)(2,1)S(1)} %copy-done.2, bf16[1,256,2048]{2,1,0:T(8,128)(2,1)S(1)} %copy-done.3), custom_call_target="tpu_custom_call" | custom-call | flops 100000000 | bytes 1048576 | tf_op jit(solution)/shard_map/pallas_call | solution.py:300
  32.4 4.1 %all-to-all-start.1 = ((bf16[32,8,256]{2,1,0:T(8,128)(2,1)}), bf16[32,8,256]{2,1,0:T(8,128)(2,1)S(1)}, u32[]{:S(2)}, u32[]{:S(2)}) async-start(bf16[32,8,256]{2,1,0:T(8,128)(2,1)} %bitcast.5), calls=%async_computation.1 | async-start | bytes 262144 | tf_op jit(solution)/shard_map/all_to_all | solution.py:307
  36.5 0.9 %select_reduce_fusion = f32[16,2]{0,1:T(2,128)S(1)} fusion(f32[16,32]{1,0:T(8,128)} %fusion.1, s32[16,2]{0,1:T(2,128)S(1)} %copy-done.8), kind=kLoop, calls=%fused_computation.1 | loop fusion | flops 3040 | bytes 2304 | tf_op jit(solution)/shard_map/reduce_sum | solution.py:283
  37.4 0.1 copy.28
  37.5 0.1 rev.3
  37.5 0.7 %divide_multiply_fusion.weight_ref = f32[16,2]{1,0:T(8,128)S(1)} fusion(f32[16,2]{1,0:T(8,128)S(1)} %copy.28, f32[16,2]{1,0:T(8,128)S(1)} %rev.3, f32[16]{0:T(128)} %broadcast_divide_fusion), kind=kLoop, calls=%fused_computation.3 | loop fusion | flops 160 | bytes 448 | tf_op jit(solution)/shard_map/mul | solution.py:284
  38.3 6.4 %all-to-all-done.1 = bf16[32,8,256]{2,1,0:T(8,128)(2,1)S(1)} async-done(((bf16[32,8,256]{2,1,0:T(8,128)(2,1)}), bf16[32,8,256]{2,1,0:T(8,128)(2,1)S(1)}, u32[]{:S(2)}, u32[]{:S(2)}) %all-to-all-start.1) | async-done | bytes 131104 | tf_op jit(solution)/shard_map/all_to_all | solution.py:307
  44.7 0.5 shard_map.179
  45.2 0.3 collective-permute-start.1
  45.5 1.0 %collective-permute-done.1.other_ref = f32[16,128]{1,0:T(8,128)S(1)} collective-permute-done((f32[16,128]{1,0:T(8,128)S(1)}, f32[16,128]{1,0:T(8,128)S(1)}, u32[]{:S(2)}, u32[]{:S(2)}) %collective-permute-start.1) | collective-permute-done | bytes 8224 | tf_op jit(solution)/shard_map/ppermute | solution.py:21
  46.4 0.8 %shard_map.180 = bf16[16,1024]{1,0:T(8,128)(2,1)} custom-call(s32[1]{0:T(128)} %bitcast.pair_ref, f32[16,1024]{1,0:T(8,128)S(1)} %get-tuple-element.27.blend_ref, f32[16,128]{1,0:T(8,128)S(1)} %get-tuple-element.28.own_ref, f32[16,128]{1,0:T(8,128)S(1)} %collective-permute-done.1.other_ref, f32[2,2048]{1,0:T(2,128)S(1)} %copy-done.6, f32[2,2048]{1,0:T(2,128)S(1)} %copy-done.7), custom_call_target="tpu_custom_call" | custom-call | flops 1000000 | bytes 1048576 | tf_op jit(solution)/shard_map/pallas_call | solution.py:321
  (3 shorter events, 0.0 us)
Async XLA Ops:
  0.6 27.6 %copy-start = (bf16[2048,32]{0,1:T(8,128)(2,1)S(1)}, bf16[2048,32]{0,1:T(8,128)(2,1)}, u32[]{:S(2)}) copy-start(bf16[2048,32]{0,1:T(8,128)(2,1)} %param.29) | copy-start | bytes 393220
  0.7 7.7 %copy-start.8 = (s32[16,2]{0,1:T(2,128)S(1)}, s32[16,2]{0,1:T(2,128)}, u32[]{:S(2)}) copy-start(s32[16,2]{0,1:T(2,128)} %param.30) | copy-start | bytes 388
  0.7 8.8 %copy-start.4 = (bf16[16,2048]{1,0:T(8,128)(2,1)S(1)}, bf16[16,2048]{1,0:T(8,128)(2,1)}, u32[]{:S(2)}) copy-start(bf16[16,2048]{1,0:T(8,128)(2,1)} %tokens_ref.3) | copy-start | bytes 196612
  0.7 8.8 %copy-start.6 = (f32[2,2048]{1,0:T(2,128)S(1)}, f32[2,2048]{1,0:T(2,128)}, u32[]{:S(2)}) copy-start(f32[2,2048]{1,0:T(2,128)} %gain_ref.3) | copy-start | bytes 49156
  0.7 8.8 %copy-start.7 = (f32[2,2048]{1,0:T(2,128)S(1)}, f32[2,2048]{1,0:T(2,128)}, u32[]{:S(2)}) copy-start(f32[2,2048]{1,0:T(2,128)} %bias_ref.3) | copy-start | bytes 49156
  0.7 22.3 %copy-start.9 = (bf16[2048,4]{0,1:T(4,128)(2,1)S(1)}, bf16[2048,4]{0,1:T(4,128)(2,1)}, u32[]{:S(2)}) copy-start(bf16[2048,4]{0,1:T(4,128)(2,1)} %param.28) | copy-start | bytes 49156
  7.8 1.7 %collective-permute-start = (bf16[16,2048]{1,0:T(8,128)(2,1)}, bf16[16,2048]{1,0:T(8,128)(2,1)S(1)}, u32[]{:S(2)}, u32[]{:S(2)}) collective-permute-start(bf16[16,2048]{1,0:T(8,128)(2,1)} %get-tuple-element.19.own_ref), channel_id=1, source_target_pairs={{0,1},{1,0},{2,3},{3,2},{4,5},{5,4},{6,7},{7,6},{8,9},{9,8},{10,11... | collective-permute-start | bytes 196616 | tf_op jit(solution)/shard_map/ppermute | solution.py:21
  9.5 0.8 %copy-start.5 = (bf16[16,2048]{1,0:T(8,128)(2,1)S(1)}, bf16[16,2048]{1,0:T(8,128)(2,1)}, u32[]{:S(2)}) copy-start(bf16[16,2048]{1,0:T(8,128)(2,1)} %get-tuple-element.19.own_ref) | copy-start | bytes 196612
  14.8 16.0 %all-to-all-start = ((bf16[16,8,512]{2,1,0:T(8,128)(2,1)}), bf16[16,8,512]{2,1,0:T(8,128)(2,1)S(1)}, u32[]{:S(2)}, u32[]{:S(2)}) async-start(bf16[16,8,512]{2,1,0:T(8,128)(2,1)} %bitcast.3), calls=%async_computation | async-start | bytes 262144 | tf_op jit(solution)/shard_map/all_to_all | solution.py:293
  23.2 7.6 %copy-start.1 = (bf16[1,2048,256]{2,1,0:T(8,128)(2,1)S(1)}, bf16[1,2048,256]{2,1,0:T(8,128)(2,1)}, u32[]{:S(2)}) copy-start(bf16[1,2048,256]{2,1,0:T(8,128)(2,1)} %gate_ref.1) | copy-start | bytes 3145732
  23.2 7.6 %copy-start.2 = (bf16[1,2048,256]{2,1,0:T(8,128)(2,1)S(1)}, bf16[1,2048,256]{2,1,0:T(8,128)(2,1)}, u32[]{:S(2)}) copy-start(bf16[1,2048,256]{2,1,0:T(8,128)(2,1)} %up_ref.1) | copy-start | bytes 3145732
  23.2 7.6 %copy-start.3 = (bf16[1,256,2048]{2,1,0:T(8,128)(2,1)S(1)}, bf16[1,256,2048]{2,1,0:T(8,128)(2,1)}, u32[]{:S(2)}) copy-start(bf16[1,256,2048]{2,1,0:T(8,128)(2,1)} %down_ref.1) | copy-start | bytes 3145732
  32.4 12.3 %all-to-all-start.1 = ((bf16[32,8,256]{2,1,0:T(8,128)(2,1)}), bf16[32,8,256]{2,1,0:T(8,128)(2,1)S(1)}, u32[]{:S(2)}, u32[]{:S(2)}) async-start(bf16[32,8,256]{2,1,0:T(8,128)(2,1)} %bitcast.5), calls=%async_computation.1 | async-start | bytes 262144 | tf_op jit(solution)/shard_map/all_to_all | solution.py:307
  45.2 1.2 %collective-permute-start.1 = (f32[16,128]{1,0:T(8,128)S(1)}, f32[16,128]{1,0:T(8,128)S(1)}, u32[]{:S(2)}, u32[]{:S(2)}) collective-permute-start(f32[16,128]{1,0:T(8,128)S(1)} %get-tuple-element.28.own_ref), channel_id=1, source_target_pairs={{0,1},{1,0},{2,3},{3,2},{4,5},{5,4},{6,7},{7,6},{8,9},{9,8},{10,11... | collective-permute-start | bytes 24584 | tf_op jit(solution)/shard_map/ppermute | solution.py:21

commit v4 on v3

--- a/solution.py
+++ b/solution.py
@@ -42,10 +42,12 @@
     raw = dot32(tokens_ref[...], d_buf[...])
     log_sig = jnp.minimum(raw, 0.0) - jnp.log(1.0 + jnp.exp(-jnp.abs(raw)))
     decay = jnp.exp(log_sig / 16.0)
-    decay_ref[...] = decay
+    for h in range(heads):
+        decay_ref[:, h, :] = decay[:, h * key_dim : (h + 1) * key_dim]
     copies[2].wait()
     keys = dot32(tokens_ref[...], k_buf[...])
-    key_ref[...] = keys
+    for h in range(heads):
+        key_ref[:, h, :] = keys[:, h * key_dim : (h + 1) * key_dim]
     scaled = queries * decay
     copies[3].wait()
     for h in range(heads):
@@ -56,7 +58,8 @@
             )
     copies[4].wait()
     values = dot32(tokens_ref[...], v_buf[...])
-    value_ref[...] = values
+    for h in range(heads):
+        value_ref[:, h, :] = values[:, h * value_dim : (h + 1) * value_dim]
     copies[5].wait()
     gates = dot32(tokens_ref[...], g_buf[...])
     gates = gates * jax.nn.sigmoid(gates)
@@ -80,9 +83,9 @@
         functools.partial(mix_kernel, key_dim, value_dim),
         out_shape=(
             jax.ShapeDtypeStruct((rows, wo.shape[1]), jnp.bfloat16),
-            jax.ShapeDtypeStruct((rows, wk.shape[1]), f32),
-            jax.ShapeDtypeStruct((rows, wd.shape[1]), f32),
-            jax.ShapeDtypeStruct((rows, wv.shape[1]), f32),
+            jax.ShapeDtypeStruct((rows, heads, key_dim), f32),
+            jax.ShapeDtypeStruct((rows, heads, key_dim), f32),
+            jax.ShapeDtypeStruct((rows, heads, value_dim), f32),
         ),
         in_specs=[in_vmem] * 2 + [in_hbm] * 7,
         out_specs=[in_vmem] * 4,
@@ -93,7 +96,7 @@
             pltpu.VMEM((heads, rows, value_dim), f32),
             pltpu.SemaphoreType.DMA((7,)),
         ],
-        compiler_params=pltpu.CompilerParams(vmem_limit_bytes=60 * mib),
+        compiler_params=pltpu.CompilerParams(vmem_limit_bytes=53 * mib),
         cost_estimate=pl.CostEstimate(flops=200_000_000, bytes_accessed=14 * mib, transcendentals=0),
     )(tokens, gain.reshape(1, -1), wq, wd, wk, wv, wg, state, wo)
 
@@ -286,9 +289,9 @@
         (decay_rate, key_rows, value_rows, outgoing)
     )
     new_state = (
-        late_decay.reshape(row_count, heads_here, key_dim, 1) * recurrent_state
-        + late_keys.reshape(row_count, heads_here, key_dim, 1)
-        * late_values.reshape(row_count, heads_here, 1, value_dim)
+        late_decay[..., None] * recurrent_state
+        + late_keys[..., None]
+        * late_values[:, :, None, :]
     )
     arrived = lax.all_to_all(
         outgoing.reshape(ep_count, cells, model_width // pieces), "ep", split_axis=0, concat_axis=0, tiled=True

time: 47.7 us -> 44.2 us (0.927)
  local copies, waits for them, and re-layouts: 4.66 us -> 3.12 us
  Pallas kernels: 10.9 us -> 9.48 us
    mul x3 -> x0, local copies, waits for them, and re-layouts: 3.45 us -> none  [the longest x2 2.11 us: on_device(): late_keys.reshape(row_count, heads_here, key_dim, 1)]
    unnamed x21 -> x27, local copies, waits for them, and re-layouts: 0.97 us -> 2.87 us
    pallas_call x1, Pallas kernels: 7.08 us -> 5.58 us  [mix(): pl.pallas_call(functools.partial(mix_kernel, key_dim, value_dim), out_sha...]
  transfers between devices with their start and end apart: 4 -> 4, of which waited for: 4 -> 4; matrix products, arithmetic and copies ran while one was open for 17% -> 18% of each run, Pallas kernels for 0% -> 0%
where the time goes in v4:
time: 44.2 us; the launch traced here: 43.8 us
  starting transfers between devices  13 us (29%)
  waiting for transfers between devices  10 us (23%)
  Pallas kernels  9.48 us (21%)
  other arithmetic  6.53 us (15%)
  local copies, waits for them, and re-layouts  3.12 us (7%)
  matrix products  0.91 us (2%)
  between operations  0.76 us (2%)
    all_to_all x1, starting transfers between devices, on_device(): lax.all_to_all(outgoing.reshape(ep_count, cells, model_width // pieces),...  8.2 us
    all_to_all x1, waiting for transfers between devices, on_device(): lax.all_to_all(results.reshape(device_count, cells, narrow), ('ep', 'tp')...  6.48 us
    pallas_call x1, Pallas kernels, mix(): pl.pallas_call(functools.partial(mix_kernel, key_dim, value_dim), out_sha...  5.58 us
    add x1, other arithmetic, on_device(): late_decay[..., None] * recurrent_state  4.39 us
    all_to_all x1, starting transfers between devices, on_device(): lax.all_to_all(results.reshape(device_count, cells, narrow), ('ep', 'tp')...  4.03 us
    unnamed x27, local copies, waits for them, and re-layouts  2.87 us
    all_to_all x1, waiting for transfers between devices, on_device(): lax.all_to_all(outgoing.reshape(ep_count, cells, model_width // pieces),...  1.87 us
    ppermute x2, waiting for transfers between devices, swapped(): lax.ppermute(values, 'tp', [(i, (i + 1) % count) for i in range(count)])  1.67 us
  transfers between devices with their start and end apart: 4, of which 4 were waited for; matrix products, arithmetic and copies ran while one was open for 18% of the time, Pallas kernels for 0%

profile of v4, /device:TPU:0, one launch (start us, length us, event | category | flops | bytes accessed | tf_op | source)
XLA Modules:
  0.0 43.8 jit_solution(6292451922226504785)
XLA Ops:
  0.6 0.0 copy-start
  0.7 0.0 copy-start.4
  0.7 0.9 %copy-done.4 = bf16[16,2048]{1,0:T(8,128)(2,1)S(1)} copy-done((bf16[16,2048]{1,0:T(8,128)(2,1)S(1)}, bf16[16,2048]{1,0:T(8,128)(2,1)}, u32[]{:S(2)}) %copy-start.4) | copy-done | bytes 65560
  1.5 0.0 copy-start.10
  1.5 0.7 %copy-done.10 = f32[256]{0:T(256)S(1)} copy-done((f32[256]{0:T(256)S(1)}, f32[256]{0:T(256)}, u32[]{:S(2)}) %copy-start.10) | copy-done | bytes 1048
  2.2 0.0 copy-start.11
  2.2 0.0 copy-start.5
  2.2 0.0 copy-start.6
  2.2 0.0 copy-start.12
  2.2 5.6 %shard_map.176 = (bf16[16,2048]{1,0:T(8,128)(2,1)S(1)}, f32[16,2,128]{2,1,0:T(2,128)S(1)}, f32[16,2,128]{2,1,0:T(2,128)S(1)}, f32[16,2,256]{2,1,0:T(2,128)S(1)}) custom-call(bf16[16,2048]{1,0:T(8,128)(2,1)S(1)} %copy-done.4, f32[1,256]{1,0:T(1,128)S(1)} %bitcast.15, bf16[2048,256]{1,0:T(8,128)(2,1)} %wq.1, bf16[2048,256]{1,0:T(8,128)(2,1)} %wd.1, ...), custom_call_target="tpu_custom_call" | custom-call | flops 200000000 | bytes 14680064 | tf_op jit(solution)/shard_map/pallas_call | solution.py:82
  7.8 0.0 copy-start.8
  7.8 0.6 %copy-done.8 = f32[16,2,128]{2,1,0:T(2,128)} copy-done((f32[16,2,128]{2,1,0:T(2,128)}, f32[16,2,128]{2,1,0:T(2,128)S(1)}, u32[]{:S(2)}) %copy-start.8) | copy-done | bytes 16408
  8.4 0.0 copy-start.9
  8.4 0.6 %copy-done.9 = f32[16,2,128]{2,1,0:T(2,128)} copy-done((f32[16,2,128]{2,1,0:T(2,128)}, f32[16,2,128]{2,1,0:T(2,128)S(1)}, u32[]{:S(2)}) %copy-start.9) | copy-done | bytes 16408
  9.0 0.5 %collective-permute-start = (bf16[16,2048]{1,0:T(8,128)(2,1)S(1)}, bf16[16,2048]{1,0:T(8,128)(2,1)S(1)}, u32[]{:S(2)}, u32[]{:S(2)}) collective-permute-start(bf16[16,2048]{1,0:T(8,128)(2,1)S(1)} %get-tuple-element.19.own_ref), channel_id=1, source_target_pairs={{0,1},{1,0},{2,3},{3,2},{4,5},{5,4},{6,7},{7,6},{8,9},{9,8},{10,11... | collective-permute-start | bytes 196616 | tf_op jit(solution)/shard_map/ppermute | solution.py:21
  9.5 0.0 copy-done.11
  9.5 0.1 copy.26.routes_ref
  9.6 0.1 tile.10.lanes_ref
  9.7 0.7 %collective-permute-done.other_ref = bf16[16,2048]{1,0:T(8,128)(2,1)S(1)} collective-permute-done((bf16[16,2048]{1,0:T(8,128)(2,1)S(1)}, bf16[16,2048]{1,0:T(8,128)(2,1)S(1)}, u32[]{:S(2)}, u32[]{:S(2)}) %collective-permute-start) | collective-permute-done | bytes 65568 | tf_op jit(solution)/shard_map/ppermute | solution.py:21
  10.4 0.0 copy-done.5
  10.4 0.0 copy-done.6
  10.4 0.0 copy-done.7
  10.4 1.0 %shard_map.177 = (bf16[16,2048]{1,0:T(8,128)(2,1)S(1)}, bf16[128,512]{1,0:T(8,128)(2,1)}) custom-call(s32[1]{0:T(128)} %bitcast.pair_ref, bf16[16,2048]{1,0:T(8,128)(2,1)S(1)} %get-tuple-element.19.own_ref, bf16[16,2048]{1,0:T(8,128)(2,1)S(1)} %collective-permute-done.other_ref, bf16[16,2048]{1,0:T(8,128)(2,1)S(1)} %copy-done.5, f32[2,2048]{1,0:T(2,128)S(1)} %copy-done.6, ...), custom_call_target="tpu_custom_call" | custom-call | flops 20000000 | bytes 1048576 | tf_op jit(solution)/shard_map/pallas_call | solution.py:265
  11.5 8.2 %all-to-all-start = ((bf16[16,8,512]{2,1,0:T(8,128)(2,1)}), bf16[16,8,512]{2,1,0:T(8,128)(2,1)S(1)}, u32[]{:S(2)}, u32[]{:S(2)}) async-start(bf16[16,8,512]{2,1,0:T(8,128)(2,1)} %bitcast.3), calls=%async_computation | async-start | bytes 262144 | tf_op jit(solution)/shard_map/all_to_all | solution.py:296
  19.7 0.0 copy-done.12
  19.7 0.1 select_reduce_fusion.1
  19.9 0.0 copy-start.1
  19.9 0.0 copy-start.2
  19.9 0.0 copy-start.3
  19.9 4.4 %multiply_add_fusion = f32[16,2,128,256]{3,2,1,0:T(8,128)} fusion(f32[16,2,128,256]{3,2,1,0:T(8,128)} %state.1, f32[16,2,256]{2,1,0:T(2,128)S(1)} %get-tuple-element.24, f32[16,2,128]{2,1,0:T(2,128)} %copy-done.8, f32[16,2,128]{2,1,0:T(2,128)} %copy-done.9), kind=kLoop, calls=%fused_computation | loop fusion | flops 3145728 | bytes 8454144 | tf_op jit(solution)/shard_map/add | solution.py:292
  24.3 0.6 %broadcast_divide_fusion = f32[16]{0:T(128)} fusion(f32[16]{0:T(128)S(1)} %exponential_reduce_fusion), kind=kLoop, calls=%fused_computation.12 | loop fusion | flops 16 | bytes 128 | tf_op jit(solution)/shard_map/div | solution.py:284
  24.8 0.0 copy-done
  24.8 0.8 %fusion.1 = f32[16,32]{1,0:T(8,128)} fusion(bf16[16,2048]{1,0:T(8,128)(2,1)S(1)} %get-tuple-element.26.hidden_ref, bf16[2048,32]{0,1:T(8,128)(2,1)S(1)} %copy-done), kind=kOutput, calls=%fused_computation.13 | convolution fusion | flops 2097152 | bytes 198656 | tf_op jit(solution)/shard_map/dot_general | solution.py:280
  25.6 1.9 %all-to-all-done = bf16[16,8,512]{2,1,0:T(8,128)(2,1)S(1)} async-done(((bf16[16,8,512]{2,1,0:T(8,128)(2,1)}), bf16[16,8,512]{2,1,0:T(8,128)(2,1)S(1)}, u32[]{:S(2)}, u32[]{:S(2)}) %all-to-all-start) | async-done | bytes 131104 | tf_op jit(solution)/shard_map/all_to_all | solution.py:296
  27.5 0.0 copy-done.1
  27.5 0.0 copy-done.2
  27.5 0.0 copy-done.3
  27.5 1.6 %shard_map.178 = bf16[256,256]{1,0:T(8,128)(2,1)} custom-call(bf16[128,512]{1,0:T(8,128)(2,1)S(1)} %bitcast.14, bf16[1,2048,256]{2,1,0:T(8,128)(2,1)S(1)} %copy-done.1, bf16[1,2048,256]{2,1,0:T(8,128)(2,1)S(1)} %copy-done.2, bf16[1,256,2048]{2,1,0:T(8,128)(2,1)S(1)} %copy-done.3), custom_call_target="tpu_custom_call" | custom-call | flops 100000000 | bytes 1048576 | tf_op jit(solution)/shard_map/pallas_call | solution.py:303
  29.1 4.0 %all-to-all-start.1 = ((bf16[32,8,256]{2,1,0:T(8,128)(2,1)}), bf16[32,8,256]{2,1,0:T(8,128)(2,1)S(1)}, u32[]{:S(2)}, u32[]{:S(2)}) async-start(bf16[32,8,256]{2,1,0:T(8,128)(2,1)} %bitcast.5), calls=%async_computation.1 | async-start | bytes 262144 | tf_op jit(solution)/shard_map/all_to_all | solution.py:310
  33.2 0.9 %select_reduce_fusion = f32[16,2]{0,1:T(2,128)S(1)} fusion(f32[16,32]{1,0:T(8,128)} %fusion.1, s32[16,2]{0,1:T(2,128)S(1)} %copy-done.11), kind=kLoop, calls=%fused_computation.1 | loop fusion | flops 3040 | bytes 2304 | tf_op jit(solution)/shard_map/reduce_sum | solution.py:286
  34.0 0.1 copy.28
  34.1 0.1 rev.3
  34.2 0.7 %divide_multiply_fusion.weight_ref = f32[16,2]{1,0:T(8,128)S(1)} fusion(f32[16,2]{1,0:T(8,128)S(1)} %copy.28, f32[16,2]{1,0:T(8,128)S(1)} %rev.3, f32[16]{0:T(128)} %broadcast_divide_fusion), kind=kLoop, calls=%fused_computation.3 | loop fusion | flops 160 | bytes 448 | tf_op jit(solution)/shard_map/mul | solution.py:287
  34.9 6.5 %all-to-all-done.1 = bf16[32,8,256]{2,1,0:T(8,128)(2,1)S(1)} async-done(((bf16[32,8,256]{2,1,0:T(8,128)(2,1)}), bf16[32,8,256]{2,1,0:T(8,128)(2,1)S(1)}, u32[]{:S(2)}, u32[]{:S(2)}) %all-to-all-start.1) | async-done | bytes 131104 | tf_op jit(solution)/shard_map/all_to_all | solution.py:310
  41.4 0.5 %shard_map.179 = (f32[16,1024]{1,0:T(8,128)S(1)}, f32[16,128]{1,0:T(8,128)S(1)}) custom-call(s32[1]{0:T(128)} %bitcast.pair_ref, bf16[256,256]{1,0:T(8,128)(2,1)S(1)} %bitcast.13, s32[16,2]{1,0:T(8,128)S(1)} %copy.26.routes_ref, s32[2,64]{1,0:T(2,128)S(1)} %tile.10.lanes_ref, f32[16,2]{1,0:T(8,128)S(1)} %divide_multiply_fusion.weight_ref, ...), custom_call_target="tpu_custom_call" | custom-call | flops 20000000 | bytes 1048576 | tf_op jit(solution)/shard_map/pallas_call | solution.py:313
  41.8 0.3 collective-permute-start.1
  42.1 1.0 %collective-permute-done.1.other_ref = f32[16,128]{1,0:T(8,128)S(1)} collective-permute-done((f32[16,128]{1,0:T(8,128)S(1)}, f32[16,128]{1,0:T(8,128)S(1)}, u32[]{:S(2)}, u32[]{:S(2)}) %collective-permute-start.1) | collective-permute-done | bytes 8224 | tf_op jit(solution)/shard_map/ppermute | solution.py:21
  43.1 0.8 %shard_map.180 = bf16[16,1024]{1,0:T(8,128)(2,1)} custom-call(s32[1]{0:T(128)} %bitcast.pair_ref, f32[16,1024]{1,0:T(8,128)S(1)} %get-tuple-element.27.blend_ref, f32[16,128]{1,0:T(8,128)S(1)} %get-tuple-element.28.own_ref, f32[16,128]{1,0:T(8,128)S(1)} %collective-permute-done.1.other_ref, f32[2,2048]{1,0:T(2,128)S(1)} %copy-done.6, f32[2,2048]{1,0:T(2,128)S(1)} %copy-done.7), custom_call_target="tpu_custom_call" | custom-call | flops 1000000 | bytes 1048576 | tf_op jit(solution)/shard_map/pallas_call | solution.py:324
  (4 shorter events, 0.0 us)
Async XLA Ops:
  0.6 24.2 %copy-start = (bf16[2048,32]{0,1:T(8,128)(2,1)S(1)}, bf16[2048,32]{0,1:T(8,128)(2,1)}, u32[]{:S(2)}) copy-start(bf16[2048,32]{0,1:T(8,128)(2,1)} %param.29) | copy-start | bytes 393220
  0.7 0.9 %copy-start.4 = (bf16[16,2048]{1,0:T(8,128)(2,1)S(1)}, bf16[16,2048]{1,0:T(8,128)(2,1)}, u32[]{:S(2)}) copy-start(bf16[16,2048]{1,0:T(8,128)(2,1)} %tokens_ref.3) | copy-start | bytes 196612
  1.5 0.7 %copy-start.10 = (f32[256]{0:T(256)S(1)}, f32[256]{0:T(256)}, u32[]{:S(2)}) copy-start(f32[256]{0:T(256)} %param.24) | copy-start | bytes 3076
  2.2 7.3 %copy-start.11 = (s32[16,2]{0,1:T(2,128)S(1)}, s32[16,2]{0,1:T(2,128)}, u32[]{:S(2)}) copy-start(s32[16,2]{0,1:T(2,128)} %param.30) | copy-start | bytes 388
  2.2 8.2 %copy-start.5 = (bf16[16,2048]{1,0:T(8,128)(2,1)S(1)}, bf16[16,2048]{1,0:T(8,128)(2,1)}, u32[]{:S(2)}) copy-start(bf16[16,2048]{1,0:T(8,128)(2,1)} %tokens_ref.3) | copy-start | bytes 196612
  2.2 8.2 %copy-start.6 = (f32[2,2048]{1,0:T(2,128)S(1)}, f32[2,2048]{1,0:T(2,128)}, u32[]{:S(2)}) copy-start(f32[2,2048]{1,0:T(2,128)} %gain_ref.3) | copy-start | bytes 49156
  2.2 8.2 %copy-start.7 = (f32[2,2048]{1,0:T(2,128)S(1)}, f32[2,2048]{1,0:T(2,128)}, u32[]{:S(2)}) copy-start(f32[2,2048]{1,0:T(2,128)} %bias_ref.3) | copy-start | bytes 49156
  2.2 17.5 %copy-start.12 = (bf16[2048,4]{0,1:T(4,128)(2,1)S(1)}, bf16[2048,4]{0,1:T(4,128)(2,1)}, u32[]{:S(2)}) copy-start(bf16[2048,4]{0,1:T(4,128)(2,1)} %param.28) | copy-start | bytes 49156
  7.8 0.6 %copy-start.8 = (f32[16,2,128]{2,1,0:T(2,128)}, f32[16,2,128]{2,1,0:T(2,128)S(1)}, u32[]{:S(2)}) copy-start(f32[16,2,128]{2,1,0:T(2,128)S(1)} %get-tuple-element.23) | copy-start | bytes 49156
  8.4 0.6 %copy-start.9 = (f32[16,2,128]{2,1,0:T(2,128)}, f32[16,2,128]{2,1,0:T(2,128)S(1)}, u32[]{:S(2)}) copy-start(f32[16,2,128]{2,1,0:T(2,128)S(1)} %get-tuple-element.22) | copy-start | bytes 49156
  9.0 1.4 %collective-permute-start = (bf16[16,2048]{1,0:T(8,128)(2,1)S(1)}, bf16[16,2048]{1,0:T(8,128)(2,1)S(1)}, u32[]{:S(2)}, u32[]{:S(2)}) collective-permute-start(bf16[16,2048]{1,0:T(8,128)(2,1)S(1)} %get-tuple-element.19.own_ref), channel_id=1, source_target_pairs={{0,1},{1,0},{2,3},{3,2},{4,5},{5,4},{6,7},{7,6},{8,9},{9,8},{10,11... | collective-permute-start | bytes 196616 | tf_op jit(solution)/shard_map/ppermute | solution.py:21
  11.5 16.0 %all-to-all-start = ((bf16[16,8,512]{2,1,0:T(8,128)(2,1)}), bf16[16,8,512]{2,1,0:T(8,128)(2,1)S(1)}, u32[]{:S(2)}, u32[]{:S(2)}) async-start(bf16[16,8,512]{2,1,0:T(8,128)(2,1)} %bitcast.3), calls=%async_computation | async-start | bytes 262144 | tf_op jit(solution)/shard_map/all_to_all | solution.py:296
  19.9 7.6 %copy-start.1 = (bf16[1,2048,256]{2,1,0:T(8,128)(2,1)S(1)}, bf16[1,2048,256]{2,1,0:T(8,128)(2,1)}, u32[]{:S(2)}) copy-start(bf16[1,2048,256]{2,1,0:T(8,128)(2,1)} %gate_ref.1) | copy-start | bytes 3145732
  19.9 7.6 %copy-start.2 = (bf16[1,2048,256]{2,1,0:T(8,128)(2,1)S(1)}, bf16[1,2048,256]{2,1,0:T(8,128)(2,1)}, u32[]{:S(2)}) copy-start(bf16[1,2048,256]{2,1,0:T(8,128)(2,1)} %up_ref.1) | copy-start | bytes 3145732
  19.9 7.6 %copy-start.3 = (bf16[1,256,2048]{2,1,0:T(8,128)(2,1)S(1)}, bf16[1,256,2048]{2,1,0:T(8,128)(2,1)}, u32[]{:S(2)}) copy-start(bf16[1,256,2048]{2,1,0:T(8,128)(2,1)} %down_ref.1) | copy-start | bytes 3145732
  29.1 12.2 %all-to-all-start.1 = ((bf16[32,8,256]{2,1,0:T(8,128)(2,1)}), bf16[32,8,256]{2,1,0:T(8,128)(2,1)S(1)}, u32[]{:S(2)}, u32[]{:S(2)}) async-start(bf16[32,8,256]{2,1,0:T(8,128)(2,1)} %bitcast.5), calls=%async_computation.1 | async-start | bytes 262144 | tf_op jit(solution)/shard_map/all_to_all | solution.py:310
  41.8 1.2 %collective-permute-start.1 = (f32[16,128]{1,0:T(8,128)S(1)}, f32[16,128]{1,0:T(8,128)S(1)}, u32[]{:S(2)}, u32[]{:S(2)}) collective-permute-start(f32[16,128]{1,0:T(8,128)S(1)} %get-tuple-element.28.own_ref), channel_id=1, source_target_pairs={{0,1},{1,0},{2,3},{3,2},{4,5},{5,4},{6,7},{7,6},{8,9},{9,8},{10,11... | collective-permute-start | bytes 24584 | tf_op jit(solution)/shard_map/ppermute | solution.py:21
